TPU v7x, 32 devices: a whole 2x2x4 slice. The times are simulated.
32 devices in a mesh: kv: 16 (over z, y, x), tp: 2 (over core).
Axes of the slice: x: 2, y: 2, z: 4, core: 2. Of those that a mesh axis runs over, the one named last changes fastest.
Arguments:
- tokens: bfloat16 [64, 4096], P(None, 'kv')
- lengths: int32 [16], replicated, may hold values from 1 to 4, 28 in all
- memory: float32 [16, 16, 128, 128], P('kv', 'tp'), may hold values from -0.6 to 0.6
- norm_gain: float32 [4096], P('kv'), may hold values from 0.1 to 1.9
- w_query: bfloat16 [4096, 2048], P('kv', 'tp'), may hold values from -0.09375 to 0.09375
- w_key: bfloat16 [4096, 2048], P('kv', 'tp'), may hold values from -0.09375 to 0.09375
- w_value: bfloat16 [4096, 2048], P('kv', 'tp'), may hold values from -0.09375 to 0.09375
- w_outgate: bfloat16 [4096, 2048], P('kv', 'tp'), may hold values from -0.09375 to 0.09375
- w_alpha: bfloat16 [4096, 16], P('kv'), may hold values from -0.09375 to 0.09375
- w_beta: bfloat16 [4096, 16], P('kv'), may hold values from -0.09375 to 0.09375
- decay_log: float32 [16], P('tp'), may hold values from -4 to 0.5
- decay_bias: float32 [16], P('tp'), may hold values from -1 to 1
- head_gain: float32 [128], replicated, may hold values from 0.1 to 1.9
- w_output: bfloat16 [2048, 4096], P('tp', 'kv'), may hold values from -0.125 to 0.125
- mlp_gain: float32 [4096], P('kv'), may hold values from 0.1 to 1.9
- w_gate: bfloat16 [4096, 11264], P('kv', 'tp'), may hold values from -0.09375 to 0.09375
- w_up: bfloat16 [4096, 11264], P('kv', 'tp'), may hold values from -0.09375 to 0.09375
- w_down: bfloat16 [11264, 4096], P('tp', 'kv'), may hold values from -0.0546875 to 0.0546875
Outputs:
- layer_out: bfloat16 [64, 4096], P(None, 'kv')
- new_memory: float32 [16, 16, 128, 128], P('kv', 'tp')
Inputs may be any that keep to these rules, and one draw needn't show every extreme that they name: How many of a sequence's 4 slots hold live tokens; the live ones come first; the lengths add up to seven quarters of 16, rounded down.
All inputs are finite; a program needn't handle non-finite values.
Results may differ from a plain program's by a relative error of at most 0.012.
Values may be sent and summed in bfloat16 or wider, within the bound.
No kernel may reach another device: no remote copies, remote signals or barrier semaphores. Data moves between devices by JAX's collectives and lax.ppermute only.
A program may use at most 64 MiB of HBM per device.

v0:
```python
import jax
import jax.numpy as jnp
from jax import lax
from jax.sharding import PartitionSpec as P

D = 4096
DK = 128
DV = 128
NEW = 4


epsilon = 1e-06


def unit_rows(values):
    return values * lax.rsqrt(jnp.sum(values * values, axis=-1, keepdims=True) + epsilon)


def advance(memory, queries, key_rows, value_rows, decays, betas):
    outputs = []
    for step in range(queries.shape[1]):
        memory = jnp.exp(decays[:, step])[:, :, None, None] * memory
        predicted = jnp.einsum(
            "shde,shd->she", memory, key_rows[:, step], precision=lax.Precision.HIGHEST
        )
        correction = betas[:, step][:, :, None] * (value_rows[:, step] - predicted)
        memory = memory + key_rows[:, step][:, :, :, None] * correction[:, :, None, :]
        outputs.append(
            jnp.einsum("shde,shd->she", memory, queries[:, step], precision=lax.Precision.HIGHEST)
        )
    return (memory, jnp.stack(outputs, axis=1))


def per_device(
    tokens,
    lengths,
    memory,
    norm_gain,
    w_query,
    w_key,
    w_value,
    w_outgate,
    w_alpha,
    w_beta,
    decay_log,
    decay_bias,
    head_gain,
    w_output,
    mlp_gain,
    w_gate,
    w_up,
    w_down,
):
    total_rows = tokens.shape[0]
    kv_count = lax.axis_size("kv")
    kv_place = lax.axis_index("kv")
    tp_place = lax.axis_index("tp")
    own_rows = total_rows // kv_count
    seq_dev = memory.shape[0]
    heads_dev = memory.shape[1]
    token_f = tokens.astype(jnp.float32)
    squares = jnp.sum(token_f * token_f, axis=1)
    scaled = (token_f * norm_gain).astype(jnp.bfloat16)
    part_query = jnp.dot(scaled, w_query, preferred_element_type=jnp.float32)
    part_key = jnp.dot(scaled, w_key, preferred_element_type=jnp.float32)
    part_value = jnp.dot(scaled, w_value, preferred_element_type=jnp.float32)
    part_gate = jnp.dot(scaled, w_outgate, preferred_element_type=jnp.float32)
    part_alpha = jnp.dot(scaled, w_alpha, preferred_element_type=jnp.float32)
    part_beta = jnp.dot(scaled, w_beta, preferred_element_type=jnp.float32)
    all_squares = lax.psum(squares, "kv")
    sum_query, sum_key, sum_value, sum_gate, sum_alpha, sum_beta = (
        lax.psum_scatter(part_query, "kv", scatter_dimension=0, tiled=True),
        lax.psum_scatter(part_key, "kv", scatter_dimension=0, tiled=True),
        lax.psum_scatter(part_value, "kv", scatter_dimension=0, tiled=True),
        lax.psum_scatter(part_gate, "kv", scatter_dimension=0, tiled=True),
        lax.psum_scatter(part_alpha, "kv", scatter_dimension=0, tiled=True),
        lax.psum_scatter(part_beta, "kv", scatter_dimension=0, tiled=True),
    )
    own_squares = lax.dynamic_slice_in_dim(all_squares, kv_place * own_rows, own_rows)
    rstd = lax.rsqrt(own_squares / D + epsilon)[:, None]
    queries = (sum_query * rstd).astype(jnp.bfloat16)
    key_rows = (sum_key * rstd).astype(jnp.bfloat16)
    value_rows = (sum_value * rstd).astype(jnp.bfloat16)
    outgate = (sum_gate * rstd).astype(jnp.bfloat16)
    alphas = lax.dynamic_slice_in_dim(sum_alpha * rstd, tp_place * heads_dev, heads_dev, 1)
    beta_pre = lax.dynamic_slice_in_dim(sum_beta * rstd, tp_place * heads_dev, heads_dev, 1)
    own_lengths = lax.dynamic_slice_in_dim(lengths, kv_place * seq_dev, seq_dev)
    live = jnp.arange(NEW, dtype=jnp.int32)[None, :] < own_lengths[:, None]
    query_h = unit_rows(queries.astype(jnp.float32).reshape(seq_dev, NEW, heads_dev, DK)) * DK ** (
        -0.5
    )
    key_h = unit_rows(key_rows.astype(jnp.float32).reshape(seq_dev, NEW, heads_dev, DK))
    value_h = value_rows.astype(jnp.float32).reshape(seq_dev, NEW, heads_dev, DV)
    decays = -jnp.exp(decay_log) * jax.nn.softplus(alphas + decay_bias)
    decays = jnp.where(live[:, :, None], decays.reshape(seq_dev, NEW, heads_dev), 0.0)
    betas = jnp.where(
        live[:, :, None], jax.nn.sigmoid(beta_pre).reshape(seq_dev, NEW, heads_dev), 0.0
    )
    new_memory, attended = advance(memory, query_h, key_h, value_h, decays, betas)
    attended = attended * lax.rsqrt(jnp.mean(attended * attended, axis=-1, keepdims=True) + epsilon)
    gate_h = outgate.astype(jnp.float32).reshape(seq_dev, NEW, heads_dev, DV)
    mixed = (
        (attended * head_gain * jax.nn.silu(gate_h))
        .astype(jnp.bfloat16)
        .reshape(own_rows, heads_dev * DV)
    )
    attn_terms = jnp.dot(
        lax.all_gather(mixed, "kv", axis=0, tiled=True),
        w_output,
        preferred_element_type=jnp.float32,
    )
    attn_total = lax.psum(attn_terms, "tp")
    hidden = (token_f + attn_total).astype(jnp.bfloat16)
    hidden_f = hidden.astype(jnp.float32)
    hidden_squares = jnp.sum(hidden_f * hidden_f, axis=1)
    hscaled = (hidden_f * mlp_gain).astype(jnp.bfloat16)
    all_live = (jnp.arange(NEW, dtype=jnp.int32)[None, :] < lengths[:, None]).reshape(total_rows)
    part_gate_rows = jnp.dot(hscaled, w_gate, preferred_element_type=jnp.float32)
    part_up_rows = jnp.dot(hscaled, w_up, preferred_element_type=jnp.float32)
    gate_rows, up_rows, mlp_squares = lax.psum((part_gate_rows, part_up_rows, hidden_squares), "kv")
    rstd2 = lax.rsqrt(mlp_squares / D + epsilon)[:, None]
    active = (jax.nn.silu(gate_rows * rstd2) * (up_rows * rstd2)).astype(jnp.bfloat16)
    feed_terms = jnp.dot(active, w_down, preferred_element_type=jnp.float32)
    feed_total = lax.psum(feed_terms.astype(jnp.bfloat16), "tp").astype(jnp.float32)
    layer_out = jnp.where(all_live[:, None], hidden_f + feed_total, 0.0).astype(jnp.bfloat16)
    return (layer_out, new_memory)


def solution(mesh):
    placed = (
        P(None, "kv"),
        P(),
        P("kv", "tp", None, None),
        P("kv"),
        P("kv", "tp"),
        P("kv", "tp"),
        P("kv", "tp"),
        P("kv", "tp"),
        P("kv", None),
        P("kv", None),
        P("tp"),
        P("tp"),
        P(),
        P("tp", "kv"),
        P("kv"),
        P("kv", "tp"),
        P("kv", "tp"),
        P("tp", "kv"),
    )
    return jax.shard_map(
        per_device,
        mesh=mesh,
        in_specs=placed,
        out_specs=(P(None, "kv"), P("kv", "tp", None, None)),
        check_vma=False,
    )
```

profile of v0, /device:TPU:0, one launch (start us, length us, event | category | flops | bytes accessed | tf_op | source)
XLA Modules:
  0.0 358.6 jit_solution(645721127070048668)
XLA Ops:
  7.2 0.0 copy-start
  7.2 0.0 copy-start.3
  7.2 0.0 copy-start.7
  7.2 0.0 all-reduce.17.cloned.1.call-start
  7.3 2.1 fusion.61
  9.4 2.0 fusion.63
  11.4 0.0 copy-start.8
  11.4 0.0 copy-start.15
  11.5 0.9 fusion.65
  12.4 0.9 fusion.69
  13.3 0.0 all-reduce.17.cloned.1.call-update
  13.3 0.0 all-reduce.13.cloned.1.call-start
  13.4 0.1 fusion.38
  13.5 0.1 fusion.67
  13.6 0.1 fusion.71
  13.8 0.6 dynamic_slice.12
  14.4 0.6 iota_compare_fusion.1
  15.0 0.6 dynamic-slice
  16.3 80.4 %all-reduce.6 = (f32[64]{0:T(128)S(1)}, f32[64,16]{1,0:T(8,128)}, f32[64,16]{1,0:T(8,128)}) all-reduce(f32[64]{0:T(128)S(1)} %fusion.38, f32[64,16]{1,0:T(8,128)S(1)} %fusion.71, f32[64,16]{1,0:T(8,128)S(1)} %fusion.67), channel_id=1, replica_groups=mesh['kv'=16,'tp'=2] {'kv'}, use_global_device_ids=true, to_apply=%region_2.0 | all-reduce | flops 2112 | bytes 16896 | tf_op jit(solution)/shard_map/psum | solution.py:70
  96.7 0.1 add_rsqrt_fusion.4
  96.7 0.8 dynamic-slice_multiply_fusion.4
  97.5 0.1 select_bitcast_fusion
  97.6 32.9 %all-reduce.17.cloned.1.call-done = (f32[64,1024]{1,0:T(8,128)}, f32[64,1024]{1,0:T(8,128)}, f32[64,1024]{1,0:T(8,128)}, f32[64,1024]{1,0:T(8,128)}) async-done(((f32[64,1024]{1,0:T(8,128)}, f32[64,1024]{1,0:T(8,128)}, f32[64,1024]{1,0:T(8,128)}, f32[64,1024]{1,0:T(8,128)}), (f32[64,1024]{1,0:T(8,128)}, f32[64,1024]{1,0:T(8,128)}, f32[64,1024]{1,0:T(8,128)}, ...) | async-done | bytes 1048592
  130.5 0.9 convert_bitcast_fusion.1
  131.4 0.1 fusion.54
  131.5 0.1 bitcast_multiply_fusion.3
  131.5 0.1 fusion.52
  131.6 0.1 fusion.53
  131.7 0.6 fusion.15
  132.4 0.1 fusion.81
  132.4 0.7 fusion.13
  133.1 0.7 fusion.11
  133.8 0.1 fusion.79
  133.9 0.4 multiply_add_fusion.2
  134.3 0.6 fusion.9
  134.8 0.6 fusion.7
  135.5 0.1 fusion.77
  135.5 0.7 fusion.5
  136.2 0.7 fusion.3
  136.9 0.1 fusion.75
  137.0 0.8 multiply_add_fusion
  137.8 0.0 copy-start.4
  137.8 0.8 copy-done.4
  138.6 0.6 fusion.1
  139.1 0.1 fusion.55
  139.2 0.1 broadcast_bitcast_fusion
  139.3 0.9 fusion.73
  140.2 39.4 %all-gather = bf16[16,4,1024]{2,1,0:T(4,128)(2,1)S(1)} all-gather(bf16[1,4,1024]{2,1,0:T(4,128)(2,1)S(1)} %fusion.73), channel_id=1, replica_groups=mesh['kv'=16,'tp'=2] {'kv'}, dimensions={0}, use_global_device_ids=true | all-gather | bytes 139264 | tf_op jit(solution)/shard_map/all_gather | solution.py:108
  179.6 1.9 fusion.88
  181.5 0.0 all-reduce.13.cloned.1.call-update
  181.5 0.0 all-reduce.15.cloned.1.call-start
  181.5 13.7 %all-reduce.13.cloned.1.call-done = f32[64,256]{1,0:T(8,128)} async-done(((f32[64,256]{1,0:T(8,128)}), f32[64,256]{1,0:T(8,128)}) %all-reduce.13.cloned.1.call-update) | async-done | bytes 65552 | tf_op jit(solution)/shard_map/psum | solution.py:112
  195.2 0.9 fusion.41
  196.2 1.7 fusion.44
  198.0 0.6 copy-done.2
  198.5 1.8 fusion.46
  200.3 0.0 all-reduce.15.cloned.1.call-update
  200.3 0.1 iota_compare_fusion
  200.4 0.1 lt.49
  200.5 43.7 %psum.45 = f32[64]{0:T(128)S(1)} all-reduce(f32[64]{0:T(128)S(1)} %get-tuple-element.11), channel_id=1, replica_groups=mesh['kv'=16,'tp'=2] {'kv'}, use_global_device_ids=true, to_apply=%region_14.15 | all-reduce | flops 64 | bytes 512 | tf_op jit(solution)/shard_map/psum | solution.py:120
  244.2 100.4 %all-reduce.15.cloned.1.call-done = (f32[64,5632]{1,0:T(8,128)}, f32[64,5632]{1,0:T(8,128)}) async-done(((f32[64,5632]{1,0:T(8,128)}, f32[64,5632]{1,0:T(8,128)}), (f32[64,5632]{1,0:T(8,128)}, f32[64,5632]{1,0:T(8,128)})) %all-reduce.15.cloned.1.call-update) | async-done | bytes 2883600 | tf_op jit(solution)/shard_map/psum | solution.py:120
  344.6 3.4 convolution_convert_fusion
  347.9 3.4 psum.47
  351.3 0.7 fusion.43
  (34 shorter events, 0.2 us)
Async XLA Ops:
  7.2 189.0 %copy-start = (bf16[256,5632]{1,0:T(8,128)(2,1)S(1)}, bf16[256,5632]{1,0:T(8,128)(2,1)}, u32[]{:S(2)}) copy-start(bf16[256,5632]{1,0:T(8,128)(2,1)} %param.34) | copy-start | bytes 8650756
  7.2 4.2 %copy-start.3 = (bf16[64,256]{1,0:T(8,128)(2,1)S(1)}, bf16[64,256]{1,0:T(8,128)(2,1)}, u32[]{:S(2)}) copy-start(bf16[64,256]{1,0:T(8,128)(2,1)} %param.18) | copy-start | bytes 98308
  7.2 4.2 %copy-start.7 = (f32[256]{0:T(256)S(1)}, f32[256]{0:T(256)}, u32[]{:S(2)}) copy-start(f32[256]{0:T(256)} %param.21) | copy-start | bytes 3076
  7.2 4.2 %copy-start.5 = (bf16[256,1024]{1,0:T(8,128)(2,1)S(1)}, bf16[256,1024]{1,0:T(8,128)(2,1)}, u32[]{:S(2)}) copy-start(bf16[256,1024]{1,0:T(8,128)(2,1)} %param.24) | copy-start | bytes 1572868
  7.2 123.3 %all-reduce.17.cloned.1.call-start = ((), (), s32[]{:S(2)}) async-start(), calls=%async_computation.2 | async-start | bytes 2097152
  7.3 5.1 %copy-start.6 = (bf16[256,1024]{1,0:T(8,128)(2,1)S(1)}, bf16[256,1024]{1,0:T(8,128)(2,1)}, u32[]{:S(2)}) copy-start(bf16[256,1024]{1,0:T(8,128)(2,1)} %param.23) | copy-start | bytes 1572868
  11.4 2.1 copy-start.8
  11.4 2.2 copy-start.9
  11.4 2.3 copy-start.14
  11.4 2.3 copy-start.13
  11.4 3.6 %copy-start.15 = (u32[32]{0:T(128)S(1)}, u32[32]{0:T(128)}, u32[]{:S(2)}) copy-start(u32[32]{0:T(128)} %constant.45) | copy-start | bytes 388
  11.5 85.3 %copy-start.11 = (f32[128]{0:T(128)S(1)}, f32[128]{0:T(128)}, u32[]{:S(2)}) copy-start(f32[128]{0:T(128)} %param.30) | copy-start | bytes 1540
  11.5 86.0 %copy-start.12 = (f32[8]{0:T(128)S(1)}, f32[8]{0:T(128)}, u32[]{:S(2)}) copy-start(f32[8]{0:T(128)} %param.29) | copy-start | bytes 100
  12.4 119.3 %copy-start.1 = (f32[1,8,128,128]{3,2,1,0:T(8,128)S(1)}, f32[1,8,128,128]{3,2,1,0:T(8,128)}, u32[]{:S(2)}) copy-start(f32[1,8,128,128]{3,2,1,0:T(8,128)} %param.20) | copy-start | bytes 1572868
  13.3 181.9 %all-reduce.13.cloned.1.call-start = ((), (), s32[]{:S(2)}) async-start(), calls=%async_computation | async-start | bytes 131072 | tf_op jit(solution)/shard_map/psum | solution.py:112
  137.0 59.2 %copy-start.10 = (f32[256]{0:T(256)S(1)}, f32[256]{0:T(256)}, u32[]{:S(2)}) copy-start(f32[256]{0:T(256)} %param.32) | copy-start | bytes 3076
  137.8 0.8 copy-start.4
  181.5 163.1 %all-reduce.15.cloned.1.call-start = ((), (), s32[]{:S(2)}) async-start(), calls=%async_computation.1 | async-start | bytes 5767168 | tf_op jit(solution)/shard_map/psum | solution.py:120
  196.2 2.3 copy-start.2
Sparse Core Ops, SparseCore 0:
  14.3 116.1 all-reduce.16
  181.6 13.5 all-reduce.12
  201.0 143.5 all-reduce.14
where the time goes:
time: 359 us
  blocking collectives  167 us (47%)
  waiting for transfers between devices  147 us (41%)
  matrix products  20 us (6%)
  between operations  14.7 us (4%)
  other arithmetic  7.01 us (2%)
    psum x1, waiting for transfers between devices, per_device(): lax.psum((part_gate_rows, part_up_rows, hidden_squares), 'kv')  100 us
    psum x1, blocking collectives, per_device(): all_squares = lax.psum(squares, 'kv')  80.4 us
    psum x1, blocking collectives, per_device(): lax.psum((part_gate_rows, part_up_rows, hidden_squares), 'kv')  43.7 us
    all_gather x1, blocking collectives, per_device(): lax.all_gather(mixed, 'kv', axis=0, tiled=True)  39.4 us
    unnamed x4, waiting for transfers between devices  32.9 us
    psum x1, waiting for transfers between devices, per_device(): attn_total = lax.psum(attn_terms, 'tp')  13.7 us
  transfers between devices with their start and end apart: 3, of which 3 were waited for; matrix products, arithmetic and copies ran while one was open for 1% of the time, Pallas kernels for 0%

commit v1 on v0

v1 whole, which is shorter than its diff:
```python
import jax
import jax.numpy as jnp
from jax import lax
from jax.sharding import PartitionSpec as P

D = 4096
DK = 128
DV = 128
NEW = 4


epsilon = 1e-06


def unit_rows(values):
    return values * lax.rsqrt(jnp.sum(values * values, axis=-1, keepdims=True) + epsilon)


def advance(memory, queries, key_rows, value_rows, decays, betas):
    outputs = []
    for step in range(queries.shape[1]):
        memory = jnp.exp(decays[:, step])[:, :, None, None] * memory
        predicted = jnp.einsum(
            "shde,shd->she", memory, key_rows[:, step], precision=lax.Precision.HIGHEST
        )
        correction = betas[:, step][:, :, None] * (value_rows[:, step] - predicted)
        memory = memory + key_rows[:, step][:, :, :, None] * correction[:, :, None, :]
        outputs.append(
            jnp.einsum("shde,shd->she", memory, queries[:, step], precision=lax.Precision.HIGHEST)
        )
    return (memory, jnp.stack(outputs, axis=1))


def two_halves(values):
    high = values.astype(jnp.bfloat16)
    return high, (values - lax.reduce_precision(values, 8, 7)).astype(jnp.bfloat16)


def exchange(blocks):
    return lax.all_to_all(blocks, "kv", 0, 0)


def to_everyone(block, count):
    return lax.all_to_all(jnp.broadcast_to(block[None], (count, *block.shape)), "kv", 0, 0)


def over_tp(terms):
    if lax.axis_size("tp") == 2:
        return terms + lax.ppermute(terms, "tp", [(0, 1), (1, 0)])
    return lax.psum(terms, "tp")


def per_device(
    tokens,
    lengths,
    memory,
    norm_gain,
    w_query,
    w_key,
    w_value,
    w_outgate,
    w_alpha,
    w_beta,
    decay_log,
    decay_bias,
    head_gain,
    w_output,
    mlp_gain,
    w_gate,
    w_up,
    w_down,
):
    total_rows = tokens.shape[0]
    kv_count = lax.axis_size("kv")
    kv_place = lax.axis_index("kv")
    tp_place = lax.axis_index("tp")
    own_rows = total_rows // kv_count
    seq_dev = memory.shape[0]
    heads_dev = memory.shape[1]
    sequences = lengths.shape[0]
    width = heads_dev * DK
    packed = -(-(sequences * 7 // 4) // kv_count) * kv_count
    token_f = tokens.astype(jnp.float32)
    squares = jnp.sum(token_f * token_f, axis=1)
    scaled = (token_f * norm_gain).astype(jnp.bfloat16)
    parts = [
        jnp.dot(scaled, w, preferred_element_type=jnp.float32).astype(jnp.bfloat16)
        for w in (w_query, w_key, w_value, w_outgate)
    ]
    small = jnp.concatenate(
        [
            jnp.dot(scaled, w_alpha, preferred_element_type=jnp.float32),
            jnp.dot(scaled, w_beta, preferred_element_type=jnp.float32),
            squares[:, None],
        ],
        axis=1,
    )
    small_n = small.shape[1]
    high, low = two_halves(small)
    pad = jnp.zeros((total_rows, -(2 * small_n) % 128), jnp.bfloat16)
    sent = jnp.concatenate([*parts, high, low, pad], axis=1).reshape(kv_count, own_rows, -1)
    summed = jnp.sum(exchange(sent).astype(jnp.float32), axis=0)
    small = summed[:, 4 * width : 4 * width + small_n] + summed[:, 4 * width + small_n : 4 * width + 2 * small_n]
    heads_all = w_alpha.shape[1]
    rstd = lax.rsqrt(small[:, 2 * heads_all] / D + epsilon)[:, None]
    queries, key_rows, value_rows, outgate = (
        (summed[:, i * width : (i + 1) * width] * rstd).astype(jnp.bfloat16) for i in range(4)
    )
    alphas = lax.dynamic_slice_in_dim(small[:, :heads_all] * rstd, tp_place * heads_dev, heads_dev, 1)
    beta_pre = lax.dynamic_slice_in_dim(
        small[:, heads_all : 2 * heads_all] * rstd, tp_place * heads_dev, heads_dev, 1
    )
    own_lengths = lax.dynamic_slice_in_dim(lengths, kv_place * seq_dev, seq_dev)
    live = jnp.arange(NEW, dtype=jnp.int32)[None, :] < own_lengths[:, None]
    query_h = unit_rows(queries.astype(jnp.float32).reshape(seq_dev, NEW, heads_dev, DK)) * DK ** (
        -0.5
    )
    key_h = unit_rows(key_rows.astype(jnp.float32).reshape(seq_dev, NEW, heads_dev, DK))
    value_h = value_rows.astype(jnp.float32).reshape(seq_dev, NEW, heads_dev, DV)
    decays = -jnp.exp(decay_log) * jax.nn.softplus(alphas + decay_bias)
    decays = jnp.where(live[:, :, None], decays.reshape(seq_dev, NEW, heads_dev), 0.0)
    betas = jnp.where(
        live[:, :, None], jax.nn.sigmoid(beta_pre).reshape(seq_dev, NEW, heads_dev), 0.0
    )
    new_memory, attended = advance(memory, query_h, key_h, value_h, decays, betas)
    attended = attended * lax.rsqrt(jnp.mean(attended * attended, axis=-1, keepdims=True) + epsilon)
    gate_h = outgate.astype(jnp.float32).reshape(seq_dev, NEW, heads_dev, DV)
    mixed = (
        (attended * head_gain * jax.nn.silu(gate_h))
        .astype(jnp.bfloat16)
        .reshape(own_rows, heads_dev * DV)
    )
    order = jnp.arange(sequences, dtype=jnp.int32)
    starts = jnp.sum(jnp.where(order[None, :] < order[:, None], lengths[None, :], 0), axis=1)
    slot = jnp.arange(NEW, dtype=jnp.int32)
    place = jnp.where(slot[None, :] < lengths[:, None], starts[:, None] + slot[None, :], packed)
    pick = (jnp.arange(packed)[:, None] == place.reshape(1, total_rows)).astype(jnp.bfloat16)
    packed_tokens = jnp.dot(pick, tokens, preferred_element_type=jnp.float32)
    all_mixed = to_everyone(mixed, kv_count).reshape(total_rows, width)
    packed_mixed = jnp.dot(pick, all_mixed, preferred_element_type=jnp.float32).astype(jnp.bfloat16)
    attn_terms = jnp.dot(packed_mixed, w_output, preferred_element_type=jnp.float32)
    attn_total = over_tp(attn_terms)
    hidden = (packed_tokens + attn_total).astype(jnp.bfloat16)
    hidden_f = hidden.astype(jnp.float32)
    hidden_squares = jnp.sum(hidden_f * hidden_f, axis=1, keepdims=True)
    hscaled = (hidden_f * mlp_gain).astype(jnp.bfloat16)
    units = w_gate.shape[1]
    part_gate_rows = jnp.dot(hscaled, w_gate, preferred_element_type=jnp.float32)
    part_up_rows = jnp.dot(hscaled, w_up, preferred_element_type=jnp.float32)
    high, low = two_halves(jnp.broadcast_to(hidden_squares, (packed, 64)))
    sent = jnp.concatenate(
        [
            part_gate_rows.astype(jnp.bfloat16),
            part_up_rows.astype(jnp.bfloat16),
            high,
            low,
        ],
        axis=1,
    ).reshape(kv_count, packed // kv_count, -1)
    summed = jnp.sum(exchange(sent).astype(jnp.float32), axis=0)
    mlp_squares = summed[:, 2 * units] + summed[:, 2 * units + 64]
    rstd2 = lax.rsqrt(mlp_squares / D + epsilon)[:, None]
    active = (jax.nn.silu(summed[:, :units] * rstd2) * (summed[:, units : 2 * units] * rstd2)).astype(
        jnp.bfloat16
    )
    all_active = to_everyone(active, kv_count).reshape(packed, units)
    feed_terms = jnp.dot(all_active, w_down, preferred_element_type=jnp.float32)
    feed_total = over_tp(feed_terms.astype(jnp.bfloat16)).astype(jnp.float32)
    result = (hidden_f + feed_total).astype(jnp.bfloat16)
    layer_out = lax.dot_general(
        pick, result, (((0,), (0,)), ((), ())), preferred_element_type=jnp.float32
    ).astype(jnp.bfloat16)
    return (layer_out, new_memory)


def solution(mesh):
    placed = (
        P(None, "kv"),
        P(),
        P("kv", "tp", None, None),
        P("kv"),
        P("kv", "tp"),
        P("kv", "tp"),
        P("kv", "tp"),
        P("kv", "tp"),
        P("kv", None),
        P("kv", None),
        P("tp"),
        P("tp"),
        P(),
        P("tp", "kv"),
        P("kv"),
        P("kv", "tp"),
        P("kv", "tp"),
        P("tp", "kv"),
    )
    return jax.shard_map(
        per_device,
        mesh=mesh,
        in_specs=placed,
        out_specs=(P(None, "kv"), P("kv", "tp", None, None)),
        check_vma=False,
    )
```

time: 359 us -> 118 us (0.33)
  blocking collectives: 167 us -> 38.7 us
  waiting for transfers between devices: 147 us -> 22.1 us
  between operations: 14.7 us -> 0.9 us
  starting transfers between devices: 0.12 us -> 12.5 us
  local copies, waits for them, and re-layouts: 2.87 us -> 14.2 us
    psum x3 -> x0, blocking collectives: 127 us -> none  [the longest x1 80.4 us: per_device(): all_squares = lax.psum(squares, 'kv')]
    psum x2 -> x0, waiting for transfers between devices: 114 us -> none  [the longest x1 100 us: per_device(): lax.psum((part_gate_rows, part_up_rows, hidden_squares), 'kv')]
    all_gather x1 -> x0, blocking collectives: 39.4 us -> none  [per_device(): lax.all_gather(mixed, 'kv', axis=0, tiled=True)]
    all_to_all x0 -> x2, blocking collectives: none -> 38.7 us  [the longest x1 24.3 us: exchange(): return lax.all_to_all(blocks, 'kv', 0, 0)]
    unnamed x4 -> x0, waiting for transfers between devices: 32.9 us -> none
    all_to_all x0 -> x2, waiting for transfers between devices: none -> 19.7 us  [the longest x1 12.2 us: exchange(): return lax.all_to_all(blocks, 'kv', 0, 0)]
    all_to_all x0 -> x2, starting transfers between devices: none -> 12.4 us  [the longest x1 8.39 us: exchange(): return lax.all_to_all(blocks, 'kv', 0, 0)]
    reshape x0 -> x4, local copies, waits for them, and re-layouts: none -> 5.9 us  [the longest x1 2.75 us: per_device(): sent = jnp.concatenate([part_gate_rows.astype(jnp.bfloat16), part_up_rows...]
  transfers between devices with their start and end apart: 3 -> 4, of which waited for: 3 -> 4; matrix products, arithmetic and copies ran while one was open for 1% -> 3% of each run, Pallas kernels for 0% -> 0%
where the time goes in v1:
time: 118 us; the launch traced here: 117 us
  blocking collectives  38.7 us (33%)
  waiting for transfers between devices  22.1 us (19%)
  matrix products  20.8 us (18%)
  local copies, waits for them, and re-layouts  14.2 us (12%)
  starting transfers between devices  12.5 us (11%)
  other arithmetic  8.01 us (7%)
    all_to_all x1, blocking collectives, exchange(): return lax.all_to_all(blocks, 'kv', 0, 0)  24.3 us
    all_to_all x1, blocking collectives, to_everyone(): lax.all_to_all(jnp.broadcast_to(block[None], (count, *block.shape)), 'kv'...  14.4 us
    all_to_all x1, waiting for transfers between devices, exchange(): return lax.all_to_all(blocks, 'kv', 0, 0)  12.2 us
    all_to_all x1, starting transfers between devices, exchange(): return lax.all_to_all(blocks, 'kv', 0, 0)  8.39 us
    all_to_all x1, waiting for transfers between devices, to_everyone(): lax.all_to_all(jnp.broadcast_to(block[None], (count, *block.shape)), 'kv'...  7.5 us
    dot_general x4, matrix products, per_device(): jnp.dot(scaled, w, preferred_element_type=jnp.float32).astype(jnp.bfloat16)  7.17 us
    all_to_all x1, starting transfers between devices, to_everyone(): lax.all_to_all(jnp.broadcast_to(block[None], (count, *block.shape)), 'kv'...  4.01 us
    reshape x1, local copies, waits for them, and re-layouts, per_device(): sent = jnp.concatenate([part_gate_rows.astype(jnp.bfloat16), part_up_rows...  2.75 us
  transfers between devices with their start and end apart: 4, of which 4 were waited for; matrix products, arithmetic and copies ran while one was open for 3% of the time, Pallas kernels for 0%

profile of v1, /device:TPU:0, one launch (start us, length us, event | category | flops | bytes accessed | tf_op | source)
XLA Modules:
  0.0 117.2 jit_solution(362086937206226653)
XLA Ops:
  0.6 1.0 fusion.38
  1.7 0.1 copy.36
  1.8 0.9 fusion.65
  2.7 0.9 fusion.63
  3.6 0.1 fusion.41
  3.7 0.7 fusion.91
  4.4 1.3 %convolution_convert_fusion.5 = bf16[64,1024]{1,0:T(8,128)(2,1)S(1)} fusion(bf16[256,1024]{1,0:T(8,128)(2,1)} %param.22, bf16[64,256]{1,0:T(8,128)(2,1)} %param.18, f32[256]{0:T(256)} %param.21), kind=kOutput, calls=%fused_computation.6 | convolution fusion | flops 33669120 | bytes 689152 | tf_op jit(solution)/shard_map/dot_general | solution.py:87
  5.7 1.9 %convolution_convert_fusion.4 = bf16[64,1024]{1,0:T(8,128)(2,1)} fusion(bf16[256,1024]{1,0:T(8,128)(2,1)} %param.23, bf16[64,256]{1,0:T(8,128)(2,1)} %param.18, f32[256]{0:T(256)} %param.21), kind=kOutput, calls=%fused_computation.5 | convolution fusion | flops 33669120 | bytes 689152 | tf_op jit(solution)/shard_map/dot_general | solution.py:87
  7.6 2.0 %convolution_convert_fusion.3 = bf16[64,1024]{1,0:T(8,128)(2,1)} fusion(bf16[256,1024]{1,0:T(8,128)(2,1)} %param.24, bf16[64,256]{1,0:T(8,128)(2,1)} %param.18, f32[256]{0:T(256)} %param.21), kind=kOutput, calls=%fused_computation.4 | convolution fusion | flops 33669120 | bytes 689152 | tf_op jit(solution)/shard_map/dot_general | solution.py:87
  9.6 1.9 %convolution_convert_fusion.2 = bf16[64,1024]{1,0:T(8,128)(2,1)} fusion(bf16[256,1024]{1,0:T(8,128)(2,1)} %param.25, bf16[64,256]{1,0:T(8,128)(2,1)} %param.18, f32[256]{0:T(256)} %param.21), kind=kOutput, calls=%fused_computation.3 | convolution fusion | flops 33669120 | bytes 689152 | tf_op jit(solution)/shard_map/dot_general | solution.py:87
  11.5 0.6 broadcast_in_dim.47
  12.1 1.8 %concatenate.22 = bf16[64,4224]{1,0:T(8,128)(2,1)} concatenate(bf16[64,1024]{1,0:T(8,128)(2,1)S(1)} %convolution_convert_fusion.5, bf16[64,1024]{1,0:T(8,128)(2,1)} %convolution_convert_fusion.4, bf16[64,1024]{1,0:T(8,128)(2,1)} %convolution_convert_fusion.3, bf16[64,1024]{1,0:T(8,128)(2,1)} %convolution_convert_fusion.2, bf16[64,33]{1,0:T(8,128)(2,1)} %fusion.91, ...), dimensions={1} | concatenate | bytes 1081344 | tf_op jit(solution)/shard_map/concatenate | solution.py:101
  14.0 2.0 %reshape.483 = bf16[16,4,4224]{2,1,0:T(4,128)(2,1)} reshape(bf16[64,4224]{1,0:T(8,128)(2,1)} %concatenate.22) | data formatting | bytes 1081344 | tf_op jit(solution)/shard_map/reshape | solution.py:101
  16.0 8.4 %all-to-all-start = ((bf16[16,4,4224]{2,1,0:T(4,128)(2,1)}), bf16[16,4,4224]{2,1,0:T(4,128)(2,1)}, u32[]{:S(2)}, u32[]{:S(2)}) async-start(bf16[16,4,4224]{2,1,0:T(4,128)(2,1)} %reshape.483), calls=%async_computation | async-start | bytes 1081344 | tf_op jit(solution)/shard_map/all_to_all | solution.py:40
  24.4 1.2 %dynamic_slice.9 = s32[1]{0:T(128)} dynamic-slice(s32[16]{0:T(128)} %param.19, s32[]{:T(128)S(6)} %select_n.42), dynamic_slice_sizes={1} | dynamic-slice | bytes 12 | tf_op jit(solution)/shard_map/dynamic_slice | solution.py:113
  25.6 0.6 iota_compare_fusion.9
  26.3 0.7 exponential_negate_fusion
  26.9 0.7 broadcast_bitcast_fusion.1
  27.6 12.2 %all-to-all-done = bf16[16,4,4224]{2,1,0:T(4,128)(2,1)} async-done(((bf16[16,4,4224]{2,1,0:T(4,128)(2,1)}), bf16[16,4,4224]{2,1,0:T(4,128)(2,1)}, u32[]{:S(2)}, u32[]{:S(2)}) %all-to-all-start) | async-done | bytes 540704 | tf_op jit(solution)/shard_map/all_to_all | solution.py:40
  39.8 1.3 %convert_reduce_fusion.1 = f32[4,4224]{1,0:T(4,128)S(1)} fusion(bf16[16,4,4224]{2,1,0:T(4,128)(2,1)} %all-to-all-done), kind=kLoop, calls=%fused_computation.11 | loop fusion | flops 523776 | bytes 608256 | tf_op jit(solution)/shard_map/reduce_sum | solution.py:102
  41.2 0.2 rsqrt_reduce_fusion
  41.3 0.1 slice_multiply_fusion.6
  41.4 0.1 convert_bitcast_fusion.1
  41.5 0.1 fusion.52
  41.6 0.1 bitcast_multiply_fusion.3
  41.7 0.1 fusion.50
  41.8 0.1 fusion.51
  41.9 0.1 select_bitcast_fusion
  42.0 0.6 fusion.15
  42.7 0.7 fusion.13
  43.4 0.7 fusion.11
  44.2 0.4 multiply_add_fusion.2
  44.6 0.6 fusion.9
  45.1 0.6 fusion.7
  45.8 0.7 fusion.5
  46.5 0.7 fusion.3
  47.3 0.8 multiply_add_fusion
  48.1 0.8 copy-done.3
  48.9 0.6 fusion.1
  49.4 0.1 fusion.57
  49.6 0.1 fusion.60
  49.7 0.7 broadcast_in_dim.48
  50.4 4.0 %all-to-all-start.1 = ((bf16[16,4,1024]{2,1,0:T(4,128)(2,1)}), bf16[16,4,1024]{2,1,0:T(4,128)(2,1)S(1)}, u32[]{:S(2)}, u32[]{:S(2)}) async-start(bf16[16,4,1024]{2,1,0:T(4,128)(2,1)} %broadcast_in_dim.48), calls=%async_computation.1 | async-start | bytes 262144 | tf_op jit(solution)/shard_map/all_to_all | solution.py:44
  54.4 0.1 select_reduce_fusion
  54.5 0.1 add_select_fusion
  54.6 0.1 select_n.41
  54.7 7.5 %all-to-all-done.1 = bf16[16,4,1024]{2,1,0:T(4,128)(2,1)S(1)} async-done(((bf16[16,4,1024]{2,1,0:T(4,128)(2,1)}), bf16[16,4,1024]{2,1,0:T(4,128)(2,1)S(1)}, u32[]{:S(2)}, u32[]{:S(2)}) %all-to-all-start.1) | async-done | bytes 131104 | tf_op jit(solution)/shard_map/all_to_all | solution.py:44
  62.2 1.3 %fusion = f32[32,256]{1,0:T(8,128)S(1)} fusion(bf16[1024,256]{1,0:T(8,128)(2,1)} %param.31, bf16[64,1024]{1,0:T(8,128)(2,1)S(1)} %reshape.502, s32[64]{0:T(128)S(1)} %select_n.41), kind=kOutput, calls=%fused_computation.8 | convolution fusion | flops 21006336 | bytes 688384 | tf_op jit(solution)/shard_map/dot_general | solution.py:141
  63.7 1.2 %collective-permute-done = f32[32,256]{1,0:T(8,128)S(1)} collective-permute-done((f32[32,256]{1,0:T(8,128)S(1)}, f32[32,256]{1,0:T(8,128)S(1)}, u32[]{:S(2)}, u32[]{:S(2)}) %collective-permute-start) | collective-permute-done | bytes 32800 | tf_op jit(solution)/shard_map/ppermute | solution.py:49
  64.9 0.2 fusion.43
  65.1 0.6 convolution_convert_fusion
  65.7 1.3 %convolution_convert_fusion.1 = bf16[32,5632]{1,0:T(8,128)(2,1)} fusion(bf16[256,5632]{1,0:T(8,128)(2,1)S(1)} %copy-done.2, bf16[32,256]{1,0:T(8,128)(2,1)S(1)} %get-tuple-element.32, f32[256]{0:T(256)S(1)} %copy-done.5), kind=kOutput, calls=%fused_computation.1 | convolution fusion | flops 92479488 | bytes 3261440 | tf_op jit(solution)/shard_map/dot_general | solution.py:148
  67.2 1.9 %concatenate.23 = bf16[32,11392]{1,0:T(8,128)(2,1)} concatenate(bf16[32,5632]{1,0:T(8,128)(2,1)} %convolution_convert_fusion.1, bf16[32,5632]{1,0:T(8,128)(2,1)S(1)} %convolution_convert_fusion, bf16[32,64]{1,0:T(8,128)(2,1)S(1)} %broadcast_in_dim.49, bf16[32,64]{1,0:T(8,128)(2,1)S(1)} %broadcast_in_dim.50), dimensions={1} | concatenate | bytes 1458176 | tf_op jit(solution)/shard_map/concatenate | solution.py:151
  69.1 2.8 %reshape.503 = bf16[16,2,11392]{2,1,0:T(2,128)(2,1)} reshape(bf16[32,11392]{1,0:T(8,128)(2,1)} %concatenate.23) | data formatting | bytes 1458176 | tf_op jit(solution)/shard_map/reshape | solution.py:159
  71.8 24.3 %all_to_all.20 = bf16[16,2,11392]{2,1,0:T(2,128)(2,1)S(1)} all-to-all(bf16[16,2,11392]{2,1,0:T(2,128)(2,1)} %reshape.503), channel_id=1, replica_groups=mesh['kv'=16,'tp'=2] {'kv'}, dimensions={0} | all-to-all | bytes 1458176 | tf_op jit(solution)/shard_map/all_to_all | solution.py:40
  96.2 0.6 convert_reduce_fusion
  96.8 0.2 fusion.89
  97.0 0.1 fusion.40
  97.1 0.2 broadcast_in_dim.51
  97.3 14.4 %all_to_all.21 = bf16[16,2,5632]{2,1,0:T(2,128)(2,1)} all-to-all(bf16[16,2,5632]{2,1,0:T(2,128)(2,1)S(1)} %broadcast_in_dim.51), channel_id=1, replica_groups=mesh['kv'=16,'tp'=2] {'kv'}, dimensions={0} | all-to-all | bytes 720896 | tf_op jit(solution)/shard_map/all_to_all | solution.py:44
  111.7 1.1 reshape.504
  112.8 2.4 %convolution_convert_fusion.8 = bf16[32,256]{1,0:T(8,128)(2,1)S(1)} fusion(bf16[32,5632]{1,0:T(8,128)(2,1)S(1)} %reshape.504, bf16[5632,256]{1,0:T(8,128)(2,1)} %param.35), kind=kOutput, calls=%fused_computation.10 | convolution fusion | flops 92282880 | bytes 3260416 | tf_op jit(solution)/shard_map/dot_general | solution.py:167
  115.2 1.2 collective-permute-done.1
  116.4 0.8 convolution_convert_fusion.7
  (33 shorter events, 0.8 us)
Async XLA Ops:
  0.6 64.5 %copy-start = (bf16[256,5632]{1,0:T(8,128)(2,1)S(1)}, bf16[256,5632]{1,0:T(8,128)(2,1)}, u32[]{:S(2)}) copy-start(bf16[256,5632]{1,0:T(8,128)(2,1)} %param.34) | copy-start | bytes 8650756
  7.6 34.4 %copy-start.1 = (f32[1,8,128,128]{3,2,1,0:T(8,128)S(1)}, f32[1,8,128,128]{3,2,1,0:T(8,128)}, u32[]{:S(2)}) copy-start(f32[1,8,128,128]{3,2,1,0:T(8,128)} %param.20) | copy-start | bytes 1572868
  14.0 27.9 %copy-start.6 = (f32[8]{0:T(128)S(1)}, f32[8]{0:T(128)}, u32[]{:S(2)}) copy-start(f32[8]{0:T(128)} %param.29) | copy-start | bytes 100
  16.0 23.8 %all-to-all-start = ((bf16[16,4,4224]{2,1,0:T(4,128)(2,1)}), bf16[16,4,4224]{2,1,0:T(4,128)(2,1)}, u32[]{:S(2)}, u32[]{:S(2)}) async-start(bf16[16,4,4224]{2,1,0:T(4,128)(2,1)} %reshape.483), calls=%async_computation | async-start | bytes 1081344 | tf_op jit(solution)/shard_map/all_to_all | solution.py:40
  44.1 10.3 %copy-start.7 = (s32[16]{0:T(128)S(1)}, s32[16]{0:T(128)}, u32[]{:S(2)}) copy-start(s32[16]{0:T(128)} %param.19) | copy-start | bytes 196
  44.5 20.3 %copy-start.4 = (bf16[64,256]{1,0:T(8,128)(2,1)S(1)}, bf16[64,256]{1,0:T(8,128)(2,1)}, u32[]{:S(2)}) copy-start(bf16[64,256]{1,0:T(8,128)(2,1)} %param.18) | copy-start | bytes 98308
  44.6 20.6 %copy-start.5 = (f32[256]{0:T(256)S(1)}, f32[256]{0:T(256)}, u32[]{:S(2)}) copy-start(f32[256]{0:T(256)} %param.32) | copy-start | bytes 3076
  48.1 0.8 copy-start.3
  50.4 11.8 %all-to-all-start.1 = ((bf16[16,4,1024]{2,1,0:T(4,128)(2,1)}), bf16[16,4,1024]{2,1,0:T(4,128)(2,1)S(1)}, u32[]{:S(2)}, u32[]{:S(2)}) async-start(bf16[16,4,1024]{2,1,0:T(4,128)(2,1)} %broadcast_in_dim.48), calls=%async_computation.1 | async-start | bytes 262144 | tf_op jit(solution)/shard_map/all_to_all | solution.py:44
  63.6 2.2 %copy-start.2 = (bf16[256,5632]{1,0:T(8,128)(2,1)S(1)}, bf16[256,5632]{1,0:T(8,128)(2,1)}, u32[]{:S(2)}) copy-start(bf16[256,5632]{1,0:T(8,128)(2,1)} %param.33) | copy-start | bytes 8650756
  63.6 1.3 %collective-permute-start = (f32[32,256]{1,0:T(8,128)S(1)}, f32[32,256]{1,0:T(8,128)S(1)}, u32[]{:S(2)}, u32[]{:S(2)}) collective-permute-start(f32[32,256]{1,0:T(8,128)S(1)} %fusion), channel_id=1, source_target_pairs={{0,1},{1,0},{2,3},{3,2},{4,5},{5,4},{6,7},{7,6},{8,9},{9,8},{10,11... | collective-permute-start | bytes 98312 | tf_op jit(solution)/shard_map/ppermute | solution.py:49
  115.2 1.2 %collective-permute-start.1 = (bf16[32,256]{1,0:T(8,128)(2,1)S(1)}, bf16[32,256]{1,0:T(8,128)(2,1)S(1)}, u32[]{:S(2)}, u32[]{:S(2)}) collective-permute-start(bf16[32,256]{1,0:T(8,128)(2,1)S(1)} %convolution_convert_fusion.8), channel_id=1, source_target_pairs={{0,1},{1,0},{2,3},{3,2},{4,5},{5,4},{6,7},{7,6},{8,9},{9,8},{10,11... | collective-permute-start | bytes 49160 | tf_op jit(solution)/shard_map/ppermute | solution.py:49

commit v2 on v0

v2 whole, which is shorter than its diff:
```python
import functools

import jax
import jax.numpy as jnp
from jax import lax
from jax.experimental import pallas as pl
from jax.experimental.pallas import tpu as pltpu
from jax.sharding import PartitionSpec as P

D = 4096
DK = 128
DV = 128
NEW = 4
LANES = 128
SUBS = 8

epsilon = 1e-06

F32 = jnp.float32
BF16 = jnp.bfloat16
VMEM = pl.BlockSpec(memory_space=pltpu.VMEM)
SMEM = pl.BlockSpec(memory_space=pltpu.SMEM)


def call(body, outs, ins, limit, flops, name):
    moved = sum(x.size * x.dtype.itemsize for x in (*outs, *ins))
    return pl.pallas_call(
        body,
        out_shape=outs,
        in_specs=[SMEM if x.dtype == jnp.int32 else VMEM for x in ins],
        out_specs=[VMEM] * len(outs),
        compiler_params=pltpu.CompilerParams(vmem_limit_bytes=limit << 20),
        cost_estimate=pl.CostEstimate(flops=flops, bytes_accessed=moved, transcendentals=0),
        name=name,
    )(*ins)


def shape(dims, dtype):
    return jax.ShapeDtypeStruct(dims, dtype)


def iota(dims, axis):
    return lax.broadcasted_iota(jnp.int32, dims, axis)


def dot(a, b):
    return jnp.dot(a, b, preferred_element_type=F32)


def dot_nt(a, b):
    return lax.dot_general(a, b, (((1,), (1,)), ((), ())), preferred_element_type=F32)


def places(lengths_ref, sequence_of, slot_of):
    place = jnp.full(sequence_of.shape, -1, jnp.int32)
    start = 0
    for s in range(lengths_ref.shape[0]):
        held = lengths_ref[s]
        mine = (sequence_of == s) & (slot_of < held)
        place = jnp.where(mine, slot_of + start, place)
        start = start + held
    return place


def log2(n):
    assert n & (n - 1) == 0
    return n.bit_length() - 1


def front_kernel(tokens_ref, gain_ref, wq_ref, wk_ref, wv_ref, wg_ref, wa_ref, wb_ref, out_ref):
    total_rows = tokens_ref.shape[0]
    width = wq_ref.shape[1]
    heads = wa_ref.shape[0]
    tokens = tokens_ref[...]
    scaled = (tokens.astype(F32) * gain_ref[...]).astype(BF16)
    dims = (2 * total_rows, total_rows)
    row, col = iota(dims, 0), iota(dims, 1)
    target = lax.shift_left(lax.shift_right_logical(row, 3), 2) + (row & 3)
    hit = target == col
    upper = (row & 7) < NEW
    zero, one = jnp.zeros(dims, F32), jnp.ones(dims, F32)
    place_a = jnp.where(hit & upper, one, zero).astype(BF16)
    place_b = jnp.where(hit & ~upper, one, zero).astype(BF16)
    left = dot(place_a, scaled).astype(BF16)
    right = dot(place_b, scaled).astype(BF16)
    out_ref[:, :width] = (dot(left, wq_ref[...]) + dot(right, wk_ref[...])).astype(BF16)
    out_ref[:, width : 2 * width] = (dot(left, wv_ref[...]) + dot(right, wg_ref[...])).astype(BF16)
    both = dot(place_a + place_b, tokens)
    squares = jnp.sum(both * both, axis=1, keepdims=True)
    fill = jnp.zeros((LANES - 2 * heads, wa_ref.shape[1]), BF16)
    small = dot_nt(left + right, jnp.concatenate([wa_ref[...], wb_ref[...], fill], axis=0))
    lane = iota(small.shape, 1)
    small = jnp.where(lane == 2 * heads, jnp.broadcast_to(squares, small.shape), small)
    high = small.astype(BF16).astype(F32)
    first = (iota(small.shape, 0) & 7) < NEW
    out_ref[:, 2 * width :] = jnp.where(first, high, small - high).astype(BF16)


def row_sum(ref, start, columns):
    block = ref[:, start : start + columns].astype(F32)
    return jnp.sum(block.reshape(-1, SUBS, columns), axis=0)


def recur_kernel(
    lengths_ref, got_ref, memory_ref, log_ref, bias_ref, gain_ref, memory_out, mixed_out, unit, vals, preds, copies
):
    heads = memory_ref.shape[0]
    width = heads * DK
    all_heads = heads * lax.axis_size("tp")
    kv_place = lax.axis_index("kv")
    tp_place = lax.axis_index("tp")
    small = row_sum(got_ref, 2 * width, LANES)
    small = small + pltpu.roll(small, NEW, 0)
    rstd = lax.rsqrt(small[:, 2 * all_heads : 2 * all_heads + 1] / D + epsilon)
    small = small * rstd
    alphas = pltpu.roll(small, LANES - tp_place * heads, 1)[:, :heads]
    betas = pltpu.roll(small, LANES - all_heads - tp_place * heads, 1)[:, :heads]
    x = alphas + bias_ref[...]
    soft = jnp.maximum(x, 0.0) + jnp.log1p(jnp.exp(-jnp.abs(x)))
    decay = -jnp.exp(log_ref[...]) * soft
    slot = iota(decay.shape, 0)
    live = (slot & 3) < lengths_ref[kv_place]
    keep = jnp.exp(jnp.where(live, decay, 0.0))
    write = jnp.where(live, 1.0 / (1.0 + jnp.exp(-betas)), 0.0)
    unit[...] = jnp.zeros(unit.shape, F32)
    unit[heads * SUBS : heads * SUBS + SUBS, :heads] = jnp.where(slot < NEW, keep, write)
    factor = jnp.where(iota((SUBS, 1), 0) < NEW, DK ** (-0.5), 1.0)
    for h in range(heads):
        block = (row_sum(got_ref, h * DK, DK) * rstd).astype(BF16).astype(F32)
        norm = lax.rsqrt(jnp.sum(block * block, axis=1, keepdims=True) + epsilon)
        unit[h * SUBS : (h + 1) * SUBS, :] = block * norm * factor
        vals[h * SUBS : (h + 1) * SUBS, :] = (
            (row_sum(got_ref, width + h * DV, DV) * rstd).astype(BF16).astype(F32)
        )
    turned = unit[...].T
    for h in range(heads):
        state = memory_ref[h]
        for j in range(SUBS):
            at = h * SUBS + j
            preds[at : at + 1, :] = jnp.sum(turned[:, at : at + 1] * state, axis=0, keepdims=True)

    def rows(ref, j):
        return ref[pl.ds(j, heads, stride=SUBS), :]

    base = heads * SUBS
    queries = [rows(unit, t) for t in range(NEW)]
    keys = [rows(unit, NEW + t) for t in range(NEW)]
    keeps = [turned[:heads, base + t : base + t + 1] for t in range(NEW)]
    writes = [turned[:heads, base + NEW + t : base + NEW + t + 1] for t in range(NEW)]

    def inner(a, b):
        return jnp.sum(a * b, axis=1, keepdims=True)

    updates = []
    passed = []
    total = jnp.ones((heads, 1), F32)
    for t in range(NEW):
        total = total * keeps[t]
        passed = [p * keeps[t] for p in passed]
        said = total * rows(preds, NEW + t)
        for i in range(t):
            said = said + (passed[i] * inner(keys[i], keys[t])) * updates[i]
        updates.append(writes[t] * (rows(vals, t) - said))
        passed.append(jnp.ones((heads, 1), F32))
        out = total * rows(preds, t)
        for i in range(t + 1):
            out = out + (passed[i] * inner(keys[i], queries[t])) * updates[i]
        out = out * lax.rsqrt(jnp.mean(out * out, axis=1, keepdims=True) + epsilon)
        gate = rows(vals, NEW + t)
        silu = gate * (1.0 / (1.0 + jnp.exp(-gate)))
        copies[t * heads : (t + 1) * heads, :] = out * gain_ref[...] * silu
    final = [passed[i] * updates[i] for i in range(NEW)]
    for h in range(heads):
        state = memory_ref[h] * total[h : h + 1, :]
        for i in range(NEW):
            at = h * SUBS + NEW + i
            state = state + turned[:, at : at + 1] * final[i][h : h + 1, :]
        memory_out[h] = state
    mixed = copies[...].astype(BF16)
    for d in range(mixed_out.shape[0]):
        mixed_out[d] = mixed


def project_kernel(lengths_ref, mixed_ref, w_ref, out_ref):
    heads = w_ref.shape[0] // DV
    total = mixed_ref.shape[0]
    packed = out_ref.shape[0]
    col = iota((1, total), 1)
    place = places(
        lengths_ref,
        lax.shift_right_logical(col, log2(NEW * heads)),
        lax.shift_right_logical(col, log2(heads)) & 3,
    )
    wanted = jnp.where((col & (heads - 1)) == 0, place, -1)
    mixed = mixed_ref[...]
    row = iota((packed, total), 0)
    head_of = col & (heads - 1)
    sum_ = None
    for h in range(heads):
        wanted = jnp.where(head_of == h, place, -1)
        pick = jnp.where(row == wanted, 1.0, 0.0).astype(BF16)
        term = dot(dot(pick, mixed).astype(BF16), w_ref[h * DV : (h + 1) * DV, :])
        sum_ = term if sum_ is None else sum_ + term
    out_ref[...] = sum_


def picker(lengths_ref, packed, total_rows):
    col = iota((1, total_rows), 1)
    place = places(lengths_ref, lax.shift_right_logical(col, 2), col & 3)
    return jnp.where(iota((packed, total_rows), 0) == place, 1.0, 0.0).astype(BF16)


def blocks_of(granules, tiles, receiver):
    first = (receiver * granules) // tiles
    last = (receiver * granules + granules - 1) // tiles
    return first, last


def up_kernel(granules, extra, lengths_ref, *refs):
    *terms, tokens_ref, gain_ref, wg_ref, wu_ref, hidden_out, out_ref = refs
    packed = hidden_out.shape[0]
    pick = picker(lengths_ref, packed, tokens_ref.shape[0])
    hidden = dot(pick, tokens_ref[...])
    for term in terms:
        hidden = hidden + term[...]
    hidden = hidden.astype(BF16)
    hidden_out[...] = hidden
    hidden_f = hidden.astype(F32)
    scaled = (hidden_f * gain_ref[...]).astype(BF16)
    tiles = wg_ref.shape[1] // LANES
    row_blocks = packed // SUBS
    squares = jnp.sum(hidden_f * hidden_f, axis=1, keepdims=True)
    squares = jnp.broadcast_to(squares, (packed, LANES))
    high = squares.astype(BF16).astype(F32)
    halves = jnp.where(iota(squares.shape, 1) < LANES // 2, high, squares - high).astype(BF16)
    step = 4
    for start in range(0, tiles, step):
        stop = min(start + step, tiles)
        span = slice(start * LANES, stop * LANES)
        gate = dot(scaled, wg_ref[:, span])
        up = dot(scaled, wu_ref[:, span])
        for t in range(start, stop):
            lanes = slice((t - start) * LANES, (t - start + 1) * LANES)
            for b in range(row_blocks):
                rows = slice(b * SUBS, (b + 1) * SUBS)
                pair = jnp.concatenate([gate[rows, lanes], up[rows, lanes]], axis=0).astype(BF16)
                d, i = divmod(b * tiles + t, granules)
                out_ref[d, i * 16 : i * 16 + 16, :] = pair
    for d in range(out_ref.shape[0]):
        first, _ = blocks_of(granules, tiles, d)
        for e in range(extra):
            b = min(first + e, row_blocks - 1)
            at = granules * 16 + e * SUBS
            out_ref[d, at : at + SUBS, :] = halves[b * SUBS : (b + 1) * SUBS, :]


def active_kernel(granules, extra, tiles, got_ref, out_ref):
    senders = got_ref.shape[0]
    scales = []
    for e in range(extra):
        at = granules * 16 + e * SUBS
        squares = jnp.sum(got_ref[:, at : at + SUBS, :].astype(F32), axis=0)
        squares = squares[:, :1] + squares[:, LANES // 2 : LANES // 2 + 1]
        scales.append(lax.rsqrt(squares / D + epsilon))
    place = lax.axis_index("kv") if extra > 1 else 0
    for i in range(granules):
        pair = got_ref[0, i * 16 : i * 16 + 16, :].astype(F32)
        for s in range(1, senders):
            pair = pair + got_ref[s, i * 16 : i * 16 + 16, :].astype(F32)
        scale = scales[0]
        if extra > 1:
            ahead = lax.div(place * granules + i, tiles) - lax.div(place * granules, tiles)
            for e in range(1, extra):
                scale = jnp.where(ahead >= e, scales[e], scale)
        gate, up = pair[:SUBS] * scale, pair[SUBS:] * scale
        active = (gate * (1.0 / (1.0 + jnp.exp(-gate))) * up).astype(BF16)
        for d in range(senders):
            out_ref[d, i * SUBS : (i + 1) * SUBS, :] = active


def down_kernel(got_ref, w_ref, out_ref):
    packed = out_ref.shape[0]
    tiles = w_ref.shape[0] // LANES
    sum_ = None
    for t in range(tiles):
        parts = [
            got_ref[(b * tiles + t) * SUBS : (b * tiles + t + 1) * SUBS, :].astype(F32)
            for b in range(packed // SUBS)
        ]
        term = dot(jnp.concatenate(parts, axis=0).astype(BF16), w_ref[t * LANES : (t + 1) * LANES, :])
        sum_ = term if sum_ is None else sum_ + term
    out_ref[...] = sum_


def last_kernel(lengths_ref, *refs):
    *terms, hidden_ref, out_ref = refs
    packed = hidden_ref.shape[0]
    result = terms[0][...]
    for term in terms[1:]:
        result = result + term[...]
    result = (hidden_ref[...].astype(F32) + result).astype(BF16)
    pick = picker(lengths_ref, packed, out_ref.shape[0])
    out_ref[...] = lax.dot_general(
        pick, result, (((0,), (0,)), ((), ())), preferred_element_type=F32
    ).astype(BF16)


def exchange(blocks):
    return lax.all_to_all(blocks, "kv", 0, 0)


def over_tp(terms):
    if lax.axis_size("tp") == 2:
        return [terms, lax.ppermute(terms, "tp", [(0, 1), (1, 0)])]
    return [lax.psum(terms, "tp")]


def per_device(
    tokens,
    lengths,
    memory,
    norm_gain,
    w_query,
    w_key,
    w_value,
    w_outgate,
    w_alpha,
    w_beta,
    decay_log,
    decay_bias,
    head_gain,
    w_output,
    mlp_gain,
    w_gate,
    w_up,
    w_down,
):
    total_rows, own_width = tokens.shape
    kv = lax.axis_size("kv")
    seq_dev, heads = memory.shape[:2]
    assert seq_dev == 1
    width = heads * DK
    sequences = lengths.shape[0]
    units = w_gate.shape[1]
    packed = -(-(sequences * 7 // 4) // SUBS) * SUBS
    tiles = units // LANES
    granules = -(-(tiles * packed // SUBS) // kv)
    last_receiver = (tiles * packed // SUBS - 1) // granules
    extra = max(b - a + 1 for a, b in (blocks_of(granules, tiles, d) for d in range(last_receiver + 1)))
    columns = 2 * width + LANES

    (sent,) = call(
        front_kernel,
        [shape((2 * total_rows, columns), BF16)],
        [tokens, norm_gain[None], w_query, w_key, w_value, w_outgate, w_alpha.T, w_beta.T],
        16,
        4 * total_rows * own_width * 4 * width,
        "front",
    )
    got = exchange(sent.reshape(kv, SUBS, columns)).reshape(kv * SUBS, columns)
    new_memory, sent = pl.pallas_call(
        recur_kernel,
        out_shape=[shape((heads, DK, DV), F32), shape((kv, NEW * heads, DV), BF16)],
        in_specs=[SMEM] + [VMEM] * 5,
        out_specs=[VMEM] * 2,
        scratch_shapes=[
            pltpu.VMEM((LANES, LANES), F32),
            pltpu.VMEM((heads * SUBS, DV), F32),
            pltpu.VMEM((heads * SUBS, DV), F32),
            pltpu.VMEM((NEW * heads, DV), F32),
        ],
        compiler_params=pltpu.CompilerParams(vmem_limit_bytes=16 << 20),
        cost_estimate=pl.CostEstimate(flops=4 << 20, bytes_accessed=2 << 20, transcendentals=0),
        name="recur",
    )(lengths, got, memory[0], decay_log[None], decay_bias[None], head_gain[None])
    got = exchange(sent).reshape(kv * NEW * heads, DV)
    (attn,) = call(
        project_kernel, [shape((packed, own_width), F32)], [lengths, got, w_output], 8, 32 << 20, "project"
    )
    hidden, sent = call(
        functools.partial(up_kernel, granules, extra),
        [shape((packed, own_width), BF16), shape((kv, granules * 16 + extra * SUBS, LANES), BF16)],
        [lengths, *over_tp(attn), tokens, mlp_gain[None], w_gate, w_up],
        16,
        4 * packed * own_width * units,
        "up",
    )
    (sent,) = call(
        functools.partial(active_kernel, granules, extra, tiles),
        [shape((kv, granules * SUBS, LANES), BF16)],
        [exchange(sent)],
        8,
        1 << 20,
        "active",
    )
    got = exchange(sent).reshape(kv * granules * SUBS, LANES)
    (feed,) = call(
        down_kernel,
        [shape((packed, own_width), F32)],
        [got, w_down],
        16,
        2 * packed * own_width * units,
        "down",
    )
    (layer_out,) = call(
        last_kernel,
        [shape((total_rows, own_width), BF16)],
        [lengths, *over_tp(feed), hidden],
        8,
        1 << 20,
        "last",
    )
    return (layer_out, new_memory[None])


def solution(mesh):
    placed = (
        P(None, "kv"),
        P(),
        P("kv", "tp", None, None),
        P("kv"),
        P("kv", "tp"),
        P("kv", "tp"),
        P("kv", "tp"),
        P("kv", "tp"),
        P("kv", None),
        P("kv", None),
        P("tp"),
        P("tp"),
        P(),
        P("tp", "kv"),
        P("kv"),
        P("kv", "tp"),
        P("kv", "tp"),
        P("tp", "kv"),
    )
    return jax.shard_map(
        per_device,
        mesh=mesh,
        in_specs=placed,
        out_specs=(P(None, "kv"), P("kv", "tp", None, None)),
        check_vma=False,
    )
```

time: 359 us -> 98.3 us (0.27)
  waiting for transfers between devices: 147 us -> 2.41 us
  blocking collectives: 167 us -> 74.4 us
  matrix products: 20 us -> 0 us
  between operations: 14.7 us -> 0.76 us
  Pallas kernels: 0 us -> 10.1 us
  local copies, waits for them, and re-layouts: 2.87 us -> 9.88 us
  other arithmetic: 7.01 us -> 0 us
    psum x3 -> x0, blocking collectives: 127 us -> none  [the longest x1 80.4 us: per_device(): all_squares = lax.psum(squares, 'kv')]
    psum x2 -> x0, waiting for transfers between devices: 114 us -> none  [the longest x1 100 us: per_device(): lax.psum((part_gate_rows, part_up_rows, hidden_squares), 'kv')]
    all_to_all x0 -> x4, blocking collectives: none -> 74.4 us  [exchange(): return lax.all_to_all(blocks, 'kv', 0, 0)]
    all_gather x1 -> x0, blocking collectives: 39.4 us -> none  [per_device(): lax.all_gather(mixed, 'kv', axis=0, tiled=True)]
    unnamed x4 -> x0, waiting for transfers between devices: 32.9 us -> none
    dot_general x18 -> x0, matrix products: 20 us -> none  [the longest x1 3.35 us: per_device(): feed_terms = jnp.dot(active, w_down, preferred_element_type=jnp.float32)]
    pallas_call x0 -> x7, Pallas kernels: none -> 10.1 us  [the longest x6 5.79 us: call(): pl.pallas_call(body, out_shape=outs, in_specs=[SMEM if x.dtype == jnp.int...]
    unnamed x35 -> x38, local copies, waits for them, and re-layouts: 2.16 us -> 9.88 us
  transfers between devices with their start and end apart: 3 -> 2, of which waited for: 3 -> 2; matrix products, arithmetic and copies ran while one was open for 1% -> 0% of each run, Pallas kernels for 0% -> 0%
where the time goes in v2:
time: 98.3 us; the launch traced here: 97.5 us
  blocking collectives  74.4 us (76%)
  Pallas kernels  10.1 us (10%)
  local copies, waits for them, and re-layouts  9.88 us (10%)
  waiting for transfers between devices  2.41 us (2%)
    all_to_all x4, blocking collectives, exchange(): return lax.all_to_all(blocks, 'kv', 0, 0)  74.4 us
    unnamed x38, local copies, waits for them, and re-layouts  9.88 us
    pallas_call x6, Pallas kernels, call(): pl.pallas_call(body, out_shape=outs, in_specs=[SMEM if x.dtype == jnp.int...  5.79 us
    pallas_call x1, Pallas kernels, per_device(): pl.pallas_call(recur_kernel, out_shape=[shape((heads, DK, DV), F32), shap...  4.28 us
    ppermute x2, waiting for transfers between devices, over_tp(): return [terms, lax.ppermute(terms, 'tp', [(0, 1), (1, 0)])]  2.41 us
  transfers between devices with their start and end apart: 2, of which 2 were waited for; matrix products, arithmetic and copies ran while one was open for 0% of the time, Pallas kernels for 0%

profile of v2, /device:TPU:0, one launch (start us, length us, event | category | flops | bytes accessed | tf_op | source)
XLA Modules:
  0.0 97.5 jit_solution(727905482818187679)
XLA Ops:
  0.6 0.0 copy-start.13
  0.6 0.0 copy-start.18
  0.7 0.0 copy-start.17
  0.7 0.0 copy-start.16
  0.7 0.0 copy-start.15
  0.7 0.0 copy-start.3
  0.7 1.1 %copy-done.3 = bf16[256,1024]{1,0:T(8,128)(2,1)S(1)} copy-done((bf16[256,1024]{1,0:T(8,128)(2,1)S(1)}, bf16[256,1024]{1,0:T(8,128)(2,1)}, u32[]{:S(2)}) %copy-start.3) | copy-done | bytes 524312
  1.8 0.0 copy-start.4
  1.8 1.0 %copy-done.4 = bf16[256,1024]{1,0:T(8,128)(2,1)S(1)} copy-done((bf16[256,1024]{1,0:T(8,128)(2,1)S(1)}, bf16[256,1024]{1,0:T(8,128)(2,1)}, u32[]{:S(2)}) %copy-start.4) | copy-done | bytes 524312
  2.8 0.0 copy-start.5
  2.8 1.0 %copy-done.5 = bf16[256,1024]{1,0:T(8,128)(2,1)S(1)} copy-done((bf16[256,1024]{1,0:T(8,128)(2,1)S(1)}, bf16[256,1024]{1,0:T(8,128)(2,1)}, u32[]{:S(2)}) %copy-start.5) | copy-done | bytes 524312
  3.8 0.0 copy-start.6
  3.8 1.0 %copy-done.6 = bf16[256,1024]{1,0:T(8,128)(2,1)S(1)} copy-done((bf16[256,1024]{1,0:T(8,128)(2,1)S(1)}, bf16[256,1024]{1,0:T(8,128)(2,1)}, u32[]{:S(2)}) %copy-start.6) | copy-done | bytes 524312
  4.9 0.0 copy-start.9
  4.9 0.8 copy-done.9
  5.6 0.0 copy-start.11
  5.6 0.7 copy-done.11
  6.3 0.0 copy-start.12
  6.3 0.7 copy-done.12
  7.0 0.0 copy-start.14
  7.0 0.7 copy-done.14
  7.7 0.0 copy-start
  7.7 0.0 copy-start.1
  7.7 0.7 front.1
  8.4 25.2 %all_to_all.20 = bf16[16,8,2176]{2,1,0:T(8,128)(2,1)S(1)} all-to-all(bf16[16,8,2176]{2,1,0:T(8,128)(2,1)S(1)} %bitcast.13), channel_id=1, replica_groups=mesh['kv'=16,'tp'=2] {'kv'}, dimensions={0} | all-to-all | bytes 1114112 | tf_op jit(solution)/shard_map/all_to_all | solution.py:309
  33.6 0.0 copy-done.13
  33.6 0.0 copy-done.18
  33.6 0.0 copy-done.17
  33.6 0.0 copy-done.16
  33.6 0.0 copy-start.7
  33.7 1.0 %copy-done.7 = f32[1,8,128,128]{3,2,1,0:T(8,128)S(1)} copy-done((f32[1,8,128,128]{3,2,1,0:T(8,128)S(1)}, f32[1,8,128,128]{3,2,1,0:T(8,128)}, u32[]{:S(2)}) %copy-start.7) | copy-done | bytes 524312
  34.7 4.3 %recur.1 = (f32[8,128,128]{2,1,0:T(8,128)}, bf16[16,32,128]{2,1,0:T(8,128)(2,1)S(1)}) custom-call(s32[16]{0:T(128)S(1)} %copy-done.13, bf16[128,2176]{1,0:T(8,128)(2,1)S(1)} %bitcast.14, f32[8,128,128]{2,1,0:T(8,128)S(1)} %bitcast.16, f32[1,8]{1,0:T(1,128)S(1)} %bitcast.22, f32[1,8]{1,0:T(1,128)S(1)} %bitcast.23, f32[1,128]{1,0:T(1,128)S(1)} %bitcast.24), custom_call_target="tpu_custom_call" | custom-call | flops 4194304 | bytes 2097152 | tf_op jit(solution)/shard_map/recur/pallas_call | solution.py:361
  39.0 10.5 %all_to_all.21 = bf16[16,32,128]{2,1,0:T(8,128)(2,1)S(1)} all-to-all(bf16[16,32,128]{2,1,0:T(8,128)(2,1)S(1)} %get-tuple-element.6), channel_id=1, replica_groups=mesh['kv'=16,'tp'=2] {'kv'}, dimensions={0} | all-to-all | bytes 262144 | tf_op jit(solution)/shard_map/all_to_all | solution.py:309
  49.5 0.0 copy-start.8
  49.5 1.0 %copy-done.8 = bf16[1024,256]{1,0:T(8,128)(2,1)S(1)} copy-done((bf16[1024,256]{1,0:T(8,128)(2,1)S(1)}, bf16[1024,256]{1,0:T(8,128)(2,1)}, u32[]{:S(2)}) %copy-start.8) | copy-done | bytes 524312
  50.5 1.3 %project.1.refs_0_ = f32[32,256]{1,0:T(8,128)S(1)} custom-call(s32[16]{0:T(128)S(1)} %copy-done.13, bf16[512,128]{1,0:T(8,128)(2,1)S(1)} %bitcast.17, bf16[1024,256]{1,0:T(8,128)(2,1)S(1)} %copy-done.8), custom_call_target="tpu_custom_call" | custom-call | flops 33554432 | bytes 688192 | tf_op jit(solution)/shard_map/project/pallas_call | solution.py:27
  51.8 0.0 collective-permute-start
  51.8 1.2 %collective-permute-done.refs_1_ = f32[32,256]{1,0:T(8,128)S(1)} collective-permute-done((f32[32,256]{1,0:T(8,128)S(1)}, f32[32,256]{1,0:T(8,128)S(1)}, u32[]{:S(2)}, u32[]{:S(2)}) %collective-permute-start) | collective-permute-done | bytes 32800 | tf_op jit(solution)/shard_map/ppermute | solution.py:314
  53.0 0.0 copy-done.15
  53.0 0.0 copy-done
  53.0 0.0 copy-done.1
  53.0 0.0 copy-start.10
  53.0 0.7 copy-done.10
  53.8 1.8 %up.1 = (bf16[32,256]{1,0:T(8,128)(2,1)S(1)}, bf16[16,184,128]{2,1,0:T(8,128)(2,1)S(1)}) custom-call(s32[16]{0:T(128)S(1)} %copy-done.13, f32[32,256]{1,0:T(8,128)S(1)} %project.1.refs_0_, f32[32,256]{1,0:T(8,128)S(1)} %collective-permute-done.refs_1_, bf16[64,256]{1,0:T(8,128)(2,1)S(1)} %copy-done.10, f32[1,256]{1,0:T(1,128)S(1)} %bitcast.21, ...), custom_call_target="tpu_custom_call" | custom-call | flops 184549376 | bytes 6636608 | tf_op jit(solution)/shard_map/up/pallas_call | solution.py:27
  55.5 0.0 copy-start.2
  55.6 24.1 %all_to_all.22.got_ref = bf16[16,184,128]{2,1,0:T(8,128)(2,1)S(1)} all-to-all(bf16[16,184,128]{2,1,0:T(8,128)(2,1)S(1)} %get-tuple-element.7), channel_id=1, replica_groups=mesh['kv'=16,'tp'=2] {'kv'}, dimensions={0} | all-to-all | bytes 1507328 | tf_op jit(solution)/shard_map/all_to_all | solution.py:309
  79.6 0.2 active.1
  79.9 14.6 %all_to_all.23 = bf16[16,88,128]{2,1,0:T(8,128)(2,1)S(1)} all-to-all(bf16[16,88,128]{2,1,0:T(8,128)(2,1)S(1)} %active.1), channel_id=1, replica_groups=mesh['kv'=16,'tp'=2] {'kv'}, dimensions={0} | all-to-all | bytes 720896 | tf_op jit(solution)/shard_map/all_to_all | solution.py:309
  94.4 0.0 copy-done.2
  94.4 0.5 down.1.refs_0_
  94.9 0.0 collective-permute-start.1
  95.0 1.2 %collective-permute-done.1.refs_1_ = f32[32,256]{1,0:T(8,128)S(1)} collective-permute-done((f32[32,256]{1,0:T(8,128)S(1)}, f32[32,256]{1,0:T(8,128)S(1)}, u32[]{:S(2)}, u32[]{:S(2)}) %collective-permute-start.1) | collective-permute-done | bytes 32800 | tf_op jit(solution)/shard_map/ppermute | solution.py:314
  96.2 1.4 %last.1 = bf16[64,256]{1,0:T(8,128)(2,1)} custom-call(s32[16]{0:T(128)S(1)} %copy-done.13, f32[32,256]{1,0:T(8,128)S(1)} %down.1.refs_0_, f32[32,256]{1,0:T(8,128)S(1)} %collective-permute-done.1.refs_1_, bf16[32,256]{1,0:T(8,128)(2,1)S(1)} %get-tuple-element.8.refs_2_), custom_call_target="tpu_custom_call" | custom-call | flops 1048576 | bytes 114752 | tf_op jit(solution)/shard_map/last/pallas_call | solution.py:27
Async XLA Ops:
  0.6 33.0 %copy-start.13 = (s32[16]{0:T(128)S(1)}, s32[16]{0:T(128)}, u32[]{:S(2)}) copy-start(s32[16]{0:T(128)} %lengths_ref.7) | copy-start | bytes 196
  0.6 33.0 %copy-start.18 = (f32[128]{0:T(128)S(1)}, f32[128]{0:T(128)}, u32[]{:S(2)}) copy-start(f32[128]{0:T(128)} %param.30) | copy-start | bytes 1540
  0.7 33.0 %copy-start.17 = (f32[8]{0:T(128)S(1)}, f32[8]{0:T(128)}, u32[]{:S(2)}) copy-start(f32[8]{0:T(128)} %param.29) | copy-start | bytes 100
  0.7 33.0 %copy-start.16 = (f32[8]{0:T(128)S(1)}, f32[8]{0:T(128)}, u32[]{:S(2)}) copy-start(f32[8]{0:T(128)} %param.28) | copy-start | bytes 100
  0.7 52.3 %copy-start.15 = (f32[256]{0:T(256)S(1)}, f32[256]{0:T(256)}, u32[]{:S(2)}) copy-start(f32[256]{0:T(256)} %param.32) | copy-start | bytes 3076
  0.7 1.1 %copy-start.3 = (bf16[256,1024]{1,0:T(8,128)(2,1)S(1)}, bf16[256,1024]{1,0:T(8,128)(2,1)}, u32[]{:S(2)}) copy-start(bf16[256,1024]{1,0:T(8,128)(2,1)} %wq_ref.1) | copy-start | bytes 1572868
  1.8 1.0 %copy-start.4 = (bf16[256,1024]{1,0:T(8,128)(2,1)S(1)}, bf16[256,1024]{1,0:T(8,128)(2,1)}, u32[]{:S(2)}) copy-start(bf16[256,1024]{1,0:T(8,128)(2,1)} %wk_ref.1) | copy-start | bytes 1572868
  2.8 1.0 %copy-start.5 = (bf16[256,1024]{1,0:T(8,128)(2,1)S(1)}, bf16[256,1024]{1,0:T(8,128)(2,1)}, u32[]{:S(2)}) copy-start(bf16[256,1024]{1,0:T(8,128)(2,1)} %wv_ref.1) | copy-start | bytes 1572868
  3.8 1.0 %copy-start.6 = (bf16[256,1024]{1,0:T(8,128)(2,1)S(1)}, bf16[256,1024]{1,0:T(8,128)(2,1)}, u32[]{:S(2)}) copy-start(bf16[256,1024]{1,0:T(8,128)(2,1)} %wg_ref.1) | copy-start | bytes 1572868
  4.9 0.8 copy-start.9
  5.6 0.7 copy-start.11
  6.3 0.7 copy-start.12
  7.0 0.7 copy-start.14
  7.7 45.3 %copy-start = (bf16[256,5632]{1,0:T(8,128)(2,1)S(1)}, bf16[256,5632]{1,0:T(8,128)(2,1)}, u32[]{:S(2)}) copy-start(bf16[256,5632]{1,0:T(8,128)(2,1)} %refs_4_.1) | copy-start | bytes 8650756
  7.7 45.3 %copy-start.1 = (bf16[256,5632]{1,0:T(8,128)(2,1)S(1)}, bf16[256,5632]{1,0:T(8,128)(2,1)}, u32[]{:S(2)}) copy-start(bf16[256,5632]{1,0:T(8,128)(2,1)} %refs_5_.1) | copy-start | bytes 8650756
  33.6 1.0 %copy-start.7 = (f32[1,8,128,128]{3,2,1,0:T(8,128)S(1)}, f32[1,8,128,128]{3,2,1,0:T(8,128)}, u32[]{:S(2)}) copy-start(f32[1,8,128,128]{3,2,1,0:T(8,128)} %param.20) | copy-start | bytes 1572868
  49.5 1.0 %copy-start.8 = (bf16[1024,256]{1,0:T(8,128)(2,1)S(1)}, bf16[1024,256]{1,0:T(8,128)(2,1)}, u32[]{:S(2)}) copy-start(bf16[1024,256]{1,0:T(8,128)(2,1)} %w_ref.2) | copy-start | bytes 1572868
  51.8 1.2 %collective-permute-start = (f32[32,256]{1,0:T(8,128)S(1)}, f32[32,256]{1,0:T(8,128)S(1)}, u32[]{:S(2)}, u32[]{:S(2)}) collective-permute-start(f32[32,256]{1,0:T(8,128)S(1)} %project.1.refs_0_), channel_id=1, source_target_pairs={{0,1},{1,0},{2,3},{3,2},{4,5},{5,4},{6,7},{7,6},{8,9},{9,8},{10,11... | collective-permute-start | bytes 98312 | tf_op jit(solution)/shard_map/ppermute | solution.py:314
  53.0 0.8 copy-start.10
  55.5 38.9 %copy-start.2 = (bf16[5632,256]{1,0:T(8,128)(2,1)S(1)}, bf16[5632,256]{1,0:T(8,128)(2,1)}, u32[]{:S(2)}) copy-start(bf16[5632,256]{1,0:T(8,128)(2,1)} %w_ref.3) | copy-start | bytes 8650756
  94.9 1.2 %collective-permute-start.1 = (f32[32,256]{1,0:T(8,128)S(1)}, f32[32,256]{1,0:T(8,128)S(1)}, u32[]{:S(2)}, u32[]{:S(2)}) collective-permute-start(f32[32,256]{1,0:T(8,128)S(1)} %down.1.refs_0_), channel_id=1, source_target_pairs={{0,1},{1,0},{2,3},{3,2},{4,5},{5,4},{6,7},{7,6},{8,9},{9,8},{10,11... | collective-permute-start | bytes 98312 | tf_op jit(solution)/shard_map/ppermute | solution.py:314

commit v3 on v2

--- a/solution.py
+++ b/solution.py
@@ -19,20 +19,26 @@
 F32 = jnp.float32
 BF16 = jnp.bfloat16
 VMEM = pl.BlockSpec(memory_space=pltpu.VMEM)
-SMEM = pl.BlockSpec(memory_space=pltpu.SMEM)
-
-
-def call(body, outs, ins, limit, flops, name):
+HBM = pl.BlockSpec(memory_space=pltpu.HBM)
+
+
+def call(body, outs, ins, specs, limit, flops, name, scratch=(), out_specs=None):
     moved = sum(x.size * x.dtype.itemsize for x in (*outs, *ins))
+    ins = [pltpu.with_memory_space_constraint(x, pltpu.HBM) if s is HBM else x for x, s in zip(ins, specs)]
     return pl.pallas_call(
         body,
         out_shape=outs,
-        in_specs=[SMEM if x.dtype == jnp.int32 else VMEM for x in ins],
-        out_specs=[VMEM] * len(outs),
+        in_specs=specs,
+        out_specs=out_specs or [VMEM] * len(outs),
+        scratch_shapes=list(scratch),
         compiler_params=pltpu.CompilerParams(vmem_limit_bytes=limit << 20),
         cost_estimate=pl.CostEstimate(flops=flops, bytes_accessed=moved, transcendentals=0),
         name=name,
     )(*ins)
+
+
+def room(x):
+    return pltpu.VMEM(x.shape, x.dtype)
 
 
 def shape(dims, dtype):
@@ -67,12 +73,28 @@
     return n.bit_length() - 1
 
 
-def front_kernel(tokens_ref, gain_ref, wq_ref, wk_ref, wv_ref, wg_ref, wa_ref, wb_ref, out_ref):
+def front_kernel(heads, *refs):
+    count = 9
+    sources, (out_ref, base_ref, pick_ref, place_ref, own_ref) = refs[:count], refs[count : count + 5]
+    held, sems = refs[count + 5 : 2 * count + 5], refs[2 * count + 5]
+    copies = [pltpu.make_async_copy(a, b, sems.at[i]) for i, (a, b) in enumerate(zip(sources, held))]
+    for copy in copies:
+        copy.start()
+    lengths_ref, tokens_ref, gain_ref, wa_ref, wb_ref, wq_ref, wk_ref, wv_ref, wg_ref = held
     total_rows = tokens_ref.shape[0]
     width = wq_ref.shape[1]
-    heads = wa_ref.shape[0]
-    tokens = tokens_ref[...]
-    scaled = (tokens.astype(F32) * gain_ref[...]).astype(BF16)
+    all_heads = wa_ref.shape[0]
+    packed = pick_ref.shape[0]
+    copies[0].wait()
+    own_ref[...] = jnp.full(own_ref.shape, lengths_ref[lax.axis_index("kv")], jnp.int32)
+    col = iota(place_ref.shape, 1)
+    place_ref[...] = places(
+        lengths_ref,
+        lax.shift_right_logical(col, log2(NEW * heads)),
+        lax.shift_right_logical(col, log2(heads)) & 3,
+    )
+    pick = picker(lengths_ref, packed, total_rows)
+    pick_ref[...] = pick
     dims = (2 * total_rows, total_rows)
     row, col = iota(dims, 0), iota(dims, 1)
     target = lax.shift_left(lax.shift_right_logical(row, 3), 2) + (row & 3)
@@ -81,19 +103,28 @@
     zero, one = jnp.zeros(dims, F32), jnp.ones(dims, F32)
     place_a = jnp.where(hit & upper, one, zero).astype(BF16)
     place_b = jnp.where(hit & ~upper, one, zero).astype(BF16)
+    fill = jnp.zeros((LANES - 2 * all_heads, wa_ref.shape[1]), BF16)
+    for copy in copies[1:5]:
+        copy.wait()
+    tokens = tokens_ref[...]
+    base_ref[...] = dot(pick, tokens)
+    scaled = (tokens.astype(F32) * gain_ref[...]).astype(BF16)
     left = dot(place_a, scaled).astype(BF16)
     right = dot(place_b, scaled).astype(BF16)
-    out_ref[:, :width] = (dot(left, wq_ref[...]) + dot(right, wk_ref[...])).astype(BF16)
-    out_ref[:, width : 2 * width] = (dot(left, wv_ref[...]) + dot(right, wg_ref[...])).astype(BF16)
     both = dot(place_a + place_b, tokens)
     squares = jnp.sum(both * both, axis=1, keepdims=True)
-    fill = jnp.zeros((LANES - 2 * heads, wa_ref.shape[1]), BF16)
     small = dot_nt(left + right, jnp.concatenate([wa_ref[...], wb_ref[...], fill], axis=0))
     lane = iota(small.shape, 1)
-    small = jnp.where(lane == 2 * heads, jnp.broadcast_to(squares, small.shape), small)
+    small = jnp.where(lane == 2 * all_heads, jnp.broadcast_to(squares, small.shape), small)
     high = small.astype(BF16).astype(F32)
     first = (iota(small.shape, 0) & 7) < NEW
     out_ref[:, 2 * width :] = jnp.where(first, high, small - high).astype(BF16)
+    copies[5].wait()
+    copies[6].wait()
+    out_ref[:, :width] = (dot(left, wq_ref[...]) + dot(right, wk_ref[...])).astype(BF16)
+    copies[7].wait()
+    copies[8].wait()
+    out_ref[:, width : 2 * width] = (dot(left, wv_ref[...]) + dot(right, wg_ref[...])).astype(BF16)
 
 
 def row_sum(ref, start, columns):
@@ -102,12 +133,28 @@
 
 
 def recur_kernel(
-    lengths_ref, got_ref, memory_ref, log_ref, bias_ref, gain_ref, memory_out, mixed_out, unit, vals, preds, copies
+    own_ref,
+    got_ref,
+    memory_hbm,
+    log_ref,
+    bias_ref,
+    gain_ref,
+    memory_out,
+    mixed_out,
+    unit,
+    vals,
+    preds,
+    copies,
+    memory_ref,
+    fresh_ref,
+    sem,
+    out_sem,
 ):
     heads = memory_ref.shape[0]
+    fetch = pltpu.make_async_copy(memory_hbm, memory_ref, sem)
+    fetch.start()
     width = heads * DK
     all_heads = heads * lax.axis_size("tp")
-    kv_place = lax.axis_index("kv")
     tp_place = lax.axis_index("tp")
     small = row_sum(got_ref, 2 * width, LANES)
     small = small + pltpu.roll(small, NEW, 0)
@@ -119,7 +166,7 @@
     soft = jnp.maximum(x, 0.0) + jnp.log1p(jnp.exp(-jnp.abs(x)))
     decay = -jnp.exp(log_ref[...]) * soft
     slot = iota(decay.shape, 0)
-    live = (slot & 3) < lengths_ref[kv_place]
+    live = (slot & 3) < own_ref[:, :heads]
     keep = jnp.exp(jnp.where(live, decay, 0.0))
     write = jnp.where(live, 1.0 / (1.0 + jnp.exp(-betas)), 0.0)
     unit[...] = jnp.zeros(unit.shape, F32)
@@ -133,6 +180,7 @@
             (row_sum(got_ref, width + h * DV, DV) * rstd).astype(BF16).astype(F32)
         )
     turned = unit[...].T
+    fetch.wait()
     for h in range(heads):
         state = memory_ref[h]
         for j in range(SUBS):
@@ -151,7 +199,7 @@
     def inner(a, b):
         return jnp.sum(a * b, axis=1, keepdims=True)
 
-    updates = []
+    updates, outs = [], []
     passed = []
     total = jnp.ones((heads, 1), F32)
     for t in range(NEW):
@@ -165,41 +213,45 @@
         out = total * rows(preds, t)
         for i in range(t + 1):
             out = out + (passed[i] * inner(keys[i], queries[t])) * updates[i]
-        out = out * lax.rsqrt(jnp.mean(out * out, axis=1, keepdims=True) + epsilon)
-        gate = rows(vals, NEW + t)
-        silu = gate * (1.0 / (1.0 + jnp.exp(-gate)))
-        copies[t * heads : (t + 1) * heads, :] = out * gain_ref[...] * silu
+        outs.append(out)
     final = [passed[i] * updates[i] for i in range(NEW)]
     for h in range(heads):
         state = memory_ref[h] * total[h : h + 1, :]
         for i in range(NEW):
             at = h * SUBS + NEW + i
             state = state + turned[:, at : at + 1] * final[i][h : h + 1, :]
-        memory_out[h] = state
+        fresh_ref[h] = state
+    store = pltpu.make_async_copy(fresh_ref, memory_out, out_sem)
+    store.start()
+    for t, out in enumerate(outs):
+        out = out * lax.rsqrt(jnp.mean(out * out, axis=1, keepdims=True) + epsilon)
+        gate = rows(vals, NEW + t)
+        silu = gate * (1.0 / (1.0 + jnp.exp(-gate)))
+        copies[t * heads : (t + 1) * heads, :] = out * gain_ref[...] * silu
     mixed = copies[...].astype(BF16)
     for d in range(mixed_out.shape[0]):
         mixed_out[d] = mixed
-
-
-def project_kernel(lengths_ref, mixed_ref, w_ref, out_ref):
+    store.wait()
+
+
+def project_kernel(place_ref, mixed_ref, w_hbm, out_ref, w_ref, sem):
+    fetch = pltpu.make_async_copy(w_hbm, w_ref, sem)
+    fetch.start()
     heads = w_ref.shape[0] // DV
     total = mixed_ref.shape[0]
     packed = out_ref.shape[0]
-    col = iota((1, total), 1)
-    place = places(
-        lengths_ref,
-        lax.shift_right_logical(col, log2(NEW * heads)),
-        lax.shift_right_logical(col, log2(heads)) & 3,
-    )
-    wanted = jnp.where((col & (heads - 1)) == 0, place, -1)
+    place = place_ref[...]
+    head_of = iota((1, total), 1) & (heads - 1)
+    row = iota((packed, total), 0)
     mixed = mixed_ref[...]
-    row = iota((packed, total), 0)
-    head_of = col & (heads - 1)
+    rows = []
+    for h in range(heads):
+        pick = jnp.where(row == jnp.where(head_of == h, place, -1), 1.0, 0.0).astype(BF16)
+        rows.append(dot(pick, mixed).astype(BF16))
+    fetch.wait()
     sum_ = None
     for h in range(heads):
-        wanted = jnp.where(head_of == h, place, -1)
-        pick = jnp.where(row == wanted, 1.0, 0.0).astype(BF16)
-        term = dot(dot(pick, mixed).astype(BF16), w_ref[h * DV : (h + 1) * DV, :])
+        term = dot(rows[h], w_ref[h * DV : (h + 1) * DV, :])
         sum_ = term if sum_ is None else sum_ + term
     out_ref[...] = sum_
 
@@ -216,11 +268,10 @@
     return first, last
 
 
-def up_kernel(granules, extra, lengths_ref, *refs):
-    *terms, tokens_ref, gain_ref, wg_ref, wu_ref, hidden_out, out_ref = refs
+def up_kernel(granules, extra, *refs):
+    *terms, base_ref, gain_ref, wg_ref, wu_ref, hidden_out, out_ref = refs
     packed = hidden_out.shape[0]
-    pick = picker(lengths_ref, packed, tokens_ref.shape[0])
-    hidden = dot(pick, tokens_ref[...])
+    hidden = base_ref[...]
     for term in terms:
         hidden = hidden + term[...]
     hidden = hidden.astype(BF16)
@@ -292,16 +343,14 @@
     out_ref[...] = sum_
 
 
-def last_kernel(lengths_ref, *refs):
-    *terms, hidden_ref, out_ref = refs
-    packed = hidden_ref.shape[0]
+def last_kernel(*refs):
+    *terms, hidden_ref, pick_ref, out_ref = refs
     result = terms[0][...]
     for term in terms[1:]:
         result = result + term[...]
     result = (hidden_ref[...].astype(F32) + result).astype(BF16)
-    pick = picker(lengths_ref, packed, out_ref.shape[0])
     out_ref[...] = lax.dot_general(
-        pick, result, (((0,), (0,)), ((), ())), preferred_element_type=F32
+        pick_ref[...], result, (((0,), (0,)), ((), ())), preferred_element_type=F32
     ).astype(BF16)
 
 
@@ -349,38 +398,61 @@
     extra = max(b - a + 1 for a, b in (blocks_of(granules, tiles, d) for d in range(last_receiver + 1)))
     columns = 2 * width + LANES
 
-    (sent,) = call(
-        front_kernel,
-        [shape((2 * total_rows, columns), BF16)],
-        [tokens, norm_gain[None], w_query, w_key, w_value, w_outgate, w_alpha.T, w_beta.T],
+    operands = [lengths, tokens, norm_gain[None], w_alpha.T, w_beta.T, w_query, w_key, w_value, w_outgate]
+    sent, base, pick, place, own = call(
+        functools.partial(front_kernel, heads),
+        [
+            shape((2 * total_rows, columns), BF16),
+            shape((packed, own_width), F32),
+            shape((packed, total_rows), BF16),
+            shape((1, kv * NEW * heads), jnp.int32),
+            shape((SUBS, LANES), jnp.int32),
+        ],
+        operands,
+        [HBM] * len(operands),
         16,
         4 * total_rows * own_width * 4 * width,
         "front",
+        [pltpu.SMEM(lengths.shape, jnp.int32), *(room(x) for x in operands[1:]), pltpu.SemaphoreType.DMA((len(operands),))],
     )
     got = exchange(sent.reshape(kv, SUBS, columns)).reshape(kv * SUBS, columns)
-    new_memory, sent = pl.pallas_call(
+    new_memory, sent = call(
         recur_kernel,
-        out_shape=[shape((heads, DK, DV), F32), shape((kv, NEW * heads, DV), BF16)],
-        in_specs=[SMEM] + [VMEM] * 5,
-        out_specs=[VMEM] * 2,
-        scratch_shapes=[
+        [shape((heads, DK, DV), F32), shape((kv, NEW * heads, DV), BF16)],
+        [own, got, memory[0], decay_log[None], decay_bias[None], head_gain[None]],
+        [VMEM, VMEM, HBM, VMEM, VMEM, VMEM],
+        16,
+        4 << 30,
+        "recur",
+        [
             pltpu.VMEM((LANES, LANES), F32),
             pltpu.VMEM((heads * SUBS, DV), F32),
             pltpu.VMEM((heads * SUBS, DV), F32),
             pltpu.VMEM((NEW * heads, DV), F32),
+            pltpu.VMEM((heads, DK, DV), F32),
+            pltpu.VMEM((heads, DK, DV), F32),
+            pltpu.SemaphoreType.DMA,
+            pltpu.SemaphoreType.DMA,
         ],
-        compiler_params=pltpu.CompilerParams(vmem_limit_bytes=16 << 20),
-        cost_estimate=pl.CostEstimate(flops=4 << 20, bytes_accessed=2 << 20, transcendentals=0),
-        name="recur",
-    )(lengths, got, memory[0], decay_log[None], decay_bias[None], head_gain[None])
+        [HBM, VMEM],
+    )
     got = exchange(sent).reshape(kv * NEW * heads, DV)
     (attn,) = call(
-        project_kernel, [shape((packed, own_width), F32)], [lengths, got, w_output], 8, 32 << 20, "project"
-    )
+        project_kernel,
+        [shape((packed, own_width), F32)],
+        [place, got, w_output],
+        [VMEM, VMEM, HBM],
+        8,
+        32 << 20,
+        "project",
+        [room(w_output), pltpu.SemaphoreType.DMA],
+    )
+    terms = over_tp(attn)
     hidden, sent = call(
         functools.partial(up_kernel, granules, extra),
         [shape((packed, own_width), BF16), shape((kv, granules * 16 + extra * SUBS, LANES), BF16)],
-        [lengths, *over_tp(attn), tokens, mlp_gain[None], w_gate, w_up],
+        [*terms, base, mlp_gain[None], w_gate, w_up],
+        [VMEM] * (len(terms) + 4),
         16,
         4 * packed * own_width * units,
         "up",
@@ -389,6 +461,7 @@
         functools.partial(active_kernel, granules, extra, tiles),
         [shape((kv, granules * SUBS, LANES), BF16)],
         [exchange(sent)],
+        [VMEM],
         8,
         1 << 20,
         "active",
@@ -398,14 +471,17 @@
         down_kernel,
         [shape((packed, own_width), F32)],
         [got, w_down],
+        [VMEM] * 2,
         16,
         2 * packed * own_width * units,
         "down",
     )
+    terms = over_tp(feed)
     (layer_out,) = call(
         last_kernel,
         [shape((total_rows, own_width), BF16)],
-        [lengths, *over_tp(feed), hidden],
+        [*terms, hidden, pick],
+        [VMEM] * (len(terms) + 2),
         8,
         1 << 20,
         "last",

time: 98.3 us -> 87.7 us (0.89)
  local copies, waits for them, and re-layouts: 9.88 us -> 0.04 us
    unnamed x38 -> x14, local copies, waits for them, and re-layouts: 9.88 us -> 0.04 us
where the time goes in v3:
time: 87.7 us; the launch traced here: 87.3 us
  blocking collectives  74.1 us (84%)
  Pallas kernels  9.94 us (11%)
  waiting for transfers between devices  2.39 us (3%)
    all_to_all x4, blocking collectives, exchange(): return lax.all_to_all(blocks, 'kv', 0, 0)  74.1 us
    pallas_call x7, Pallas kernels, call(): pl.pallas_call(body, out_shape=outs, in_specs=specs, out_specs=out_specs...  9.94 us
    ppermute x2, waiting for transfers between devices, over_tp(): return [terms, lax.ppermute(terms, 'tp', [(0, 1), (1, 0)])]  2.39 us
  transfers between devices with their start and end apart: 2, of which 2 were waited for; matrix products, arithmetic and copies ran while one was open for 0% of the time, Pallas kernels for 0%

profile of v3, /device:TPU:0, one launch (start us, length us, event | category | flops | bytes accessed | tf_op | source)
XLA Modules:
  0.0 87.3 jit_solution(13757522269103240619)
XLA Ops:
  0.6 0.0 copy-start.6
  0.6 0.0 copy-start.5
  0.7 0.0 copy-start.4
  0.7 2.0 %front.1 = (bf16[128,2176]{1,0:T(8,128)(2,1)S(1)}, f32[32,256]{1,0:T(8,128)S(1)}, bf16[32,64]{1,0:T(8,128)(2,1)S(1)}, s32[1,512]{1,0:T(1,128)S(1)}, s32[8,128]{1,0:T(8,128)S(1)}) custom-call(s32[16]{0:T(128)} %refs_0_.1, bf16[64,256]{1,0:T(8,128)(2,1)} %refs_1_.1, f32[1,256]{1,0:T(1,128)} %bitcast.23, bf16[16,256]{1,0:T(8,128)(2,1)} %bitcast.21, ...), custom_call_target="tpu_custom_call" | custom-call | flops 268435456 | bytes 2747456 | tf_op jit(solution)/shard_map/front/pallas_call | solution.py:28
  2.7 25.0 %all_to_all.20 = bf16[16,8,2176]{2,1,0:T(8,128)(2,1)S(1)} all-to-all(bf16[16,8,2176]{2,1,0:T(8,128)(2,1)S(1)} %bitcast.14), channel_id=1, replica_groups=mesh['kv'=16,'tp'=2] {'kv'}, dimensions={0} | all-to-all | bytes 1114112 | tf_op jit(solution)/shard_map/all_to_all | solution.py:358
  27.6 0.0 copy-done.6
  27.6 0.0 copy-done.5
  27.6 0.0 copy-done.4
  27.6 0.0 copy-start
  27.7 0.0 copy-start.1
  27.7 0.0 copy-start.3
  27.7 3.9 %recur.1 = (f32[8,128,128]{2,1,0:T(8,128)}, bf16[16,32,128]{2,1,0:T(8,128)(2,1)S(1)}) custom-call(s32[8,128]{1,0:T(8,128)S(1)} %get-tuple-element.12.own_ref, bf16[128,2176]{1,0:T(8,128)(2,1)S(1)} %bitcast.15, f32[8,128,128]{2,1,0:T(8,128)} %bitcast.24, f32[1,8]{1,0:T(1,128)S(1)} %bitcast.18, f32[1,8]{1,0:T(1,128)S(1)} %bitcast.19, f32[1,128]{1,0:T(1,128)S(1)} %bitcast.20), custom_call_target="tpu_custom_call" | custom-call | flops 4294967296 | bytes 1741376 | tf_op jit(solution)/shard_map/recur/pallas_call | solution.py:28
  31.5 10.5 %all_to_all.21 = bf16[16,32,128]{2,1,0:T(8,128)(2,1)S(1)} all-to-all(bf16[16,32,128]{2,1,0:T(8,128)(2,1)S(1)} %get-tuple-element.14), channel_id=1, replica_groups=mesh['kv'=16,'tp'=2] {'kv'}, dimensions={0} | all-to-all | bytes 262144 | tf_op jit(solution)/shard_map/all_to_all | solution.py:358
  42.0 1.5 %project.1.refs_0_ = f32[32,256]{1,0:T(8,128)S(1)} custom-call(s32[1,512]{1,0:T(1,128)S(1)} %get-tuple-element.11.place_ref, bf16[512,128]{1,0:T(8,128)(2,1)S(1)} %bitcast.16, bf16[1024,256]{1,0:T(8,128)(2,1)} %w_hbm.1), custom_call_target="tpu_custom_call" | custom-call | flops 33554432 | bytes 690176 | tf_op jit(solution)/shard_map/project/pallas_call | solution.py:28
  43.5 0.1 collective-permute-start
  43.6 1.2 %collective-permute-done.refs_1_ = f32[32,256]{1,0:T(8,128)S(1)} collective-permute-done((f32[32,256]{1,0:T(8,128)S(1)}, f32[32,256]{1,0:T(8,128)S(1)}, u32[]{:S(2)}, u32[]{:S(2)}) %collective-permute-start) | collective-permute-done | bytes 32800 | tf_op jit(solution)/shard_map/ppermute | solution.py:363
  44.8 0.0 copy-done
  44.8 0.0 copy-done.1
  44.8 0.0 copy-done.3
  44.8 1.1 %up.1 = (bf16[32,256]{1,0:T(8,128)(2,1)S(1)}, bf16[16,184,128]{2,1,0:T(8,128)(2,1)S(1)}) custom-call(f32[32,256]{1,0:T(8,128)S(1)} %project.1.refs_0_, f32[32,256]{1,0:T(8,128)S(1)} %collective-permute-done.refs_1_, f32[32,256]{1,0:T(8,128)S(1)} %get-tuple-element.15.refs_2_, f32[1,256]{1,0:T(1,128)S(1)} %bitcast.17, bf16[256,5632]{1,0:T(8,128)(2,1)S(1)} %copy-done, ...), custom_call_target="tpu_custom_call" | custom-call | flops 184549376 | bytes 6636544 | tf_op jit(solution)/shard_map/up/pallas_call | solution.py:28
  45.9 0.0 copy-start.2
  45.9 24.1 %all_to_all.22.got_ref = bf16[16,184,128]{2,1,0:T(8,128)(2,1)S(1)} all-to-all(bf16[16,184,128]{2,1,0:T(8,128)(2,1)S(1)} %get-tuple-element.16), channel_id=1, replica_groups=mesh['kv'=16,'tp'=2] {'kv'}, dimensions={0} | all-to-all | bytes 1507328 | tf_op jit(solution)/shard_map/all_to_all | solution.py:358
  70.0 0.2 active.1
  70.2 14.6 %all_to_all.23 = bf16[16,88,128]{2,1,0:T(8,128)(2,1)S(1)} all-to-all(bf16[16,88,128]{2,1,0:T(8,128)(2,1)S(1)} %active.1), channel_id=1, replica_groups=mesh['kv'=16,'tp'=2] {'kv'}, dimensions={0} | all-to-all | bytes 720896 | tf_op jit(solution)/shard_map/all_to_all | solution.py:358
  84.8 0.0 copy-done.2
  84.8 0.5 down.1.refs_0_
  85.3 0.0 collective-permute-start.1
  85.3 1.2 %collective-permute-done.1.refs_1_ = f32[32,256]{1,0:T(8,128)S(1)} collective-permute-done((f32[32,256]{1,0:T(8,128)S(1)}, f32[32,256]{1,0:T(8,128)S(1)}, u32[]{:S(2)}, u32[]{:S(2)}) %collective-permute-start.1) | collective-permute-done | bytes 32800 | tf_op jit(solution)/shard_map/ppermute | solution.py:363
  86.5 0.8 last.1
Async XLA Ops:
  0.6 27.0 %copy-start.6 = (f32[128]{0:T(128)S(1)}, f32[128]{0:T(128)}, u32[]{:S(2)}) copy-start(f32[128]{0:T(128)} %param.30) | copy-start | bytes 1540
  0.6 27.0 %copy-start.5 = (f32[8]{0:T(128)S(1)}, f32[8]{0:T(128)}, u32[]{:S(2)}) copy-start(f32[8]{0:T(128)} %param.29) | copy-start | bytes 100
  0.7 27.0 %copy-start.4 = (f32[8]{0:T(128)S(1)}, f32[8]{0:T(128)}, u32[]{:S(2)}) copy-start(f32[8]{0:T(128)} %param.28) | copy-start | bytes 100
  27.6 17.1 %copy-start = (bf16[256,5632]{1,0:T(8,128)(2,1)S(1)}, bf16[256,5632]{1,0:T(8,128)(2,1)}, u32[]{:S(2)}) copy-start(bf16[256,5632]{1,0:T(8,128)(2,1)} %refs_4_.1) | copy-start | bytes 8650756
  27.7 17.1 %copy-start.1 = (bf16[256,5632]{1,0:T(8,128)(2,1)S(1)}, bf16[256,5632]{1,0:T(8,128)(2,1)}, u32[]{:S(2)}) copy-start(bf16[256,5632]{1,0:T(8,128)(2,1)} %refs_5_.3) | copy-start | bytes 8650756
  27.7 17.1 %copy-start.3 = (f32[256]{0:T(256)S(1)}, f32[256]{0:T(256)}, u32[]{:S(2)}) copy-start(f32[256]{0:T(256)} %param.32) | copy-start | bytes 3076
  43.5 1.3 %collective-permute-start = (f32[32,256]{1,0:T(8,128)S(1)}, f32[32,256]{1,0:T(8,128)S(1)}, u32[]{:S(2)}, u32[]{:S(2)}) collective-permute-start(f32[32,256]{1,0:T(8,128)S(1)} %project.1.refs_0_), channel_id=1, source_target_pairs={{0,1},{1,0},{2,3},{3,2},{4,5},{5,4},{6,7},{7,6},{8,9},{9,8},{10,11... | collective-permute-start | bytes 98312 | tf_op jit(solution)/shard_map/ppermute | solution.py:363
  45.9 38.9 %copy-start.2 = (bf16[5632,256]{1,0:T(8,128)(2,1)S(1)}, bf16[5632,256]{1,0:T(8,128)(2,1)}, u32[]{:S(2)}) copy-start(bf16[5632,256]{1,0:T(8,128)(2,1)} %w_ref.1) | copy-start | bytes 8650756
  85.3 1.2 %collective-permute-start.1 = (f32[32,256]{1,0:T(8,128)S(1)}, f32[32,256]{1,0:T(8,128)S(1)}, u32[]{:S(2)}, u32[]{:S(2)}) collective-permute-start(f32[32,256]{1,0:T(8,128)S(1)} %down.1.refs_0_), channel_id=1, source_target_pairs={{0,1},{1,0},{2,3},{3,2},{4,5},{5,4},{6,7},{7,6},{8,9},{9,8},{10,11... | collective-permute-start | bytes 98312 | tf_op jit(solution)/shard_map/ppermute | solution.py:363
